TPU v7x, 512 devices: a whole 4x8x8 slice. The times are simulated.
512 devices in a mesh: ep: 32 (over z, x), tp: 16 (over y, core).
Axes of the slice: x: 4, y: 8, z: 8, core: 2. Of those that a mesh axis runs over, the one named last changes fastest.
Arguments:
- mixer_in: bfloat16 [4096, 2048], P('ep'), may hold values from -6 to 6
- mixer_gain: float32 [2048], replicated, may hold values from 0.1 to 1.9
- w_value: bfloat16 [2048, 1536], P(None, 'tp'), may hold values from -0.125 to 0.125
- w_gate: bfloat16 [2048, 1536], P(None, 'tp'), may hold values from -0.125 to 0.125
- w_taps: float32 [31, 1536], P(None, 'tp'), may hold values from -3 to 3
- channel_gain: float32 [1536], P('tp'), may hold values from 0.1 to 1.9
- w_output: bfloat16 [1536, 2048], P('tp'), may hold values from -0.15625 to 0.15625
- expert_in: bfloat16 [4096, 2048], P('ep'), may hold values from -6 to 6
- expert_gain: float32 [2048], replicated, may hold values from 0 to 8
- route_experts: int32 [4096, 4], P('ep'), may hold values from 0 to 31, all different within a row; in each aligned block of 128 rows (0 to 127, 128 to 255, ...) at most 32 rows name the same one
- route_scores: float32 [4096, 4], P('ep'), may hold values from -6 to 6
- expert_gate: bfloat16 [32, 2048, 2048], P('ep', None, 'tp'), may hold values from -0.125 to 0.125
- expert_up: bfloat16 [32, 2048, 2048], P('ep', None, 'tp'), may hold values from -0.125 to 0.125
- expert_down: bfloat16 [32, 2048, 2048], P('ep', 'tp'), may hold values from -0.125 to 0.125
Outputs:
- mixer_out: bfloat16 [4096, 2048], P('ep')
- expert_out: bfloat16 [4096, 2048], P('ep')
Inputs may be any that keep to these rules, and one draw needn't show every extreme that they name: `route_experts`: each row names 4 different experts. In each aligned block of 128 rows (the rows of one index of ep) no expert is named more than 32 times, a bound that some block reaches.
All inputs are finite; a program needn't handle non-finite values.
Results may differ from a plain program's by a relative error of at most 0.02.
Values may be sent and summed in bfloat16 or wider, within the bound.
No kernel may reach another device: no remote copies, remote signals or barrier semaphores. Data moves between devices by JAX's collectives and lax.ppermute only.
A program may use at most 64 MiB of HBM per device.

v0:
```python
import jax
import jax.numpy as jnp
from jax import lax
from jax.experimental import pallas as pl
from jax.experimental.pallas import tpu as pltpu
from jax.sharding import Mesh
from jax.sharding import PartitionSpec as P

CONV_CH = 1536
CONV_W = 31
TOP_K = 4
BITS = ("y2", "y1", "y0", "c")
TP = BITS
Y = BITS[:3]
GROUP = 4
EXPERTS = 32


epsilon = 1e-05
clamp_limit = 7.0
swish_slope = 1.702


def shifted(block, axis, distance):
    devices = range(lax.axis_size(axis))
    route = [(i - distance, i) for i in devices if i - distance in devices]
    return lax.ppermute(block, axis, route)


def swapped(x, axis):
    return lax.ppermute(x, axis, [(0, 1), (1, 0)])


def exchanged(x, axis):
    return lax.all_to_all(x, axis, split_axis=0, concat_axis=0, tiled=True)


def core_half(x):
    rows, width = x.shape
    x = x.reshape(2, rows // 2, width)
    own = lax.axis_index("c")
    kept = lax.dynamic_index_in_dim(x, own, 0, keepdims=False)
    given = lax.dynamic_index_in_dim(x, 1 - own, 0, keepdims=False)
    return kept + swapped(given.astype(jnp.bfloat16), "c").astype(jnp.float32)


def totals(halves):
    size = lax.axis_size(Y)
    rows, width = halves[0].shape
    share = rows // size
    parts = [half.astype(jnp.bfloat16).reshape(size, 1, share, width) for half in halves]
    arrived = exchanged(jnp.concatenate(parts, axis=1), Y)
    summed = jnp.sum(arrived.astype(jnp.float32), axis=0).astype(jnp.bfloat16)
    gathered = exchanged(jnp.broadcast_to(summed, (size, *summed.shape)), Y)
    others = swapped(gathered, "c")
    first = lax.axis_index("c") == 0
    outs = []
    for at in range(len(halves)):
        own = gathered[:, at].reshape(rows, width)
        other = others[:, at].reshape(rows, width)
        low, high = jnp.where(first, own, other), jnp.where(first, other, own)
        outs.append(jnp.concatenate([low, high], axis=0))
    return outs


def row_norm(inputs, gains):
    widened = inputs.astype(jnp.float32)
    row_mean = jnp.mean(widened, axis=-1, keepdims=True)
    row_var = jnp.mean(jnp.square(widened - row_mean), axis=-1, keepdims=True)
    return (widened - row_mean) * lax.rsqrt(row_var + epsilon) * gains


def convolved(mixer_in, mixer_gain, w_value, w_gate, w_taps):
    normed = row_norm(mixer_in, mixer_gain).astype(jnp.bfloat16)
    values = jnp.dot(normed, w_value, preferred_element_type=jnp.float32)
    gate_pre = jnp.dot(normed, w_gate, preferred_element_type=jnp.float32)
    gated_values = (values * jax.nn.sigmoid(gate_pre)).astype(jnp.bfloat16)
    mixer_rows = gated_values.shape[0]
    reach_rows = CONV_W - 1
    earlier = shifted(gated_values[mixer_rows - reach_rows :], "ep", 1)
    extended = jnp.concatenate([earlier, gated_values], axis=0)
    conv_out = jnp.zeros(gated_values.shape, jnp.float32)
    for offset in range(CONV_W):
        conv_out = (
            conv_out + extended[offset : offset + mixer_rows].astype(jnp.float32) * w_taps[offset]
        )
    return conv_out


def projected(conv_out, channel_gain, w_output):
    sums = jnp.stack([jnp.sum(conv_out, axis=1), jnp.sum(conv_out * conv_out, axis=1)])
    everyone = lax.all_gather(sums, TP)
    sums = jnp.sum(everyone, axis=0)
    row_mean = (sums[0] / CONV_CH)[:, None]
    row_var = (sums[1] / CONV_CH)[:, None] - row_mean * row_mean
    activated = jax.nn.silu(
        (conv_out - row_mean) * lax.rsqrt(row_var + epsilon) * channel_gain
    ).astype(jnp.bfloat16)
    return jnp.dot(activated, w_output, preferred_element_type=jnp.float32)


def places(ids_ref, rows):
    names = lax.broadcasted_iota(jnp.int32, (EXPERTS, rows), 0)
    named = [ids_ref[pl.ds(k, 1), :] == names for k in range(TOP_K)]
    chosen = jnp.zeros((EXPERTS, rows), jnp.float32)
    for k in range(TOP_K):
        chosen = jnp.where(named[k], 1.0, chosen)
    earlier = lax.broadcasted_iota(jnp.int32, (rows, rows), 0)
    later = lax.broadcasted_iota(jnp.int32, (rows, rows), 1)
    before = jnp.where(earlier < later, 1.0, 0.0).astype(jnp.bfloat16)
    rank = jnp.dot(chosen.astype(jnp.bfloat16), before, preferred_element_type=jnp.float32)
    return named, jnp.where(chosen > 0.0, rank, -1.0).astype(jnp.bfloat16)


def spread_over(sent, per_expert):
    of_row = lax.broadcasted_iota(jnp.int32, (sent, EXPERTS), 0) // per_expert
    of_col = lax.broadcasted_iota(jnp.int32, (sent, EXPERTS), 1)
    return jnp.where(of_row == of_col, 1.0, 0.0).astype(jnp.bfloat16)


def taken_by(place, spread, slots, member):
    sent, rows = spread.shape[0], place.shape[1]
    slot = lax.broadcasted_iota(jnp.int32, (sent, rows), 0) % slots * GROUP + member
    return jnp.dot(spread, place, preferred_element_type=jnp.float32) == slot.astype(jnp.float32)


def front_kernel(member, x_ref, gain_ref, ids_ref, rows_ref):
    rows = x_ref.shape[0]
    sent = rows_ref.shape[0]
    slots = sent // EXPERTS
    normed = row_norm(x_ref[...], gain_ref[...]).astype(jnp.bfloat16)
    _, place = places(ids_ref, rows)
    taken = taken_by(place, spread_over(sent, slots), slots, member[0])
    select = jnp.where(taken, 1.0, 0.0).astype(jnp.bfloat16)
    rows_ref[...] = jnp.dot(select, normed, preferred_element_type=jnp.float32).astype(jnp.bfloat16)


def front(member, x, gain, ids, sent):
    _, width = x.shape
    whole = pl.BlockSpec(memory_space=pltpu.VMEM)
    return pl.pallas_call(
        front_kernel,
        in_specs=[pl.BlockSpec(memory_space=pltpu.SMEM)] + [whole] * 3,
        out_specs=whole,
        out_shape=jax.ShapeDtypeStruct((sent, width), jnp.bfloat16),
        compiler_params=pltpu.CompilerParams(vmem_limit_bytes=8 << 20),
        name="front",
    )(member.reshape(1), x, gain.reshape(1, width), ids)


def mixing_kernel(member, ids_ref, scores_ref, hi_ref, lo_ref):
    sent, rows = hi_ref.shape
    slots = sent // EXPERTS
    raised = [jnp.exp(scores_ref[pl.ds(k, 1), :]) for k in range(TOP_K)]
    total = raised[0] + raised[1] + raised[2] + raised[3]
    named, place = places(ids_ref, rows)
    weights = jnp.zeros((EXPERTS, rows), jnp.float32)
    for k in range(TOP_K):
        weights = jnp.where(named[k], raised[k] / total, weights)
    weights_hi = weights.astype(jnp.bfloat16)
    weights_lo = (weights - weights_hi.astype(jnp.float32)).astype(jnp.bfloat16)
    spread = spread_over(sent, slots)
    taken = taken_by(place, spread, slots, member[0])
    wide_hi = jnp.dot(spread, weights_hi, preferred_element_type=jnp.float32)
    wide_lo = jnp.dot(spread, weights_lo, preferred_element_type=jnp.float32)
    hi_ref[...] = jnp.where(taken, wide_hi, 0.0).astype(jnp.bfloat16)
    lo_ref[...] = jnp.where(taken, wide_lo, 0.0).astype(jnp.bfloat16)


def mixing(member, ids, scores, sent):
    rows = ids.shape[1]
    whole = pl.BlockSpec(memory_space=pltpu.VMEM)
    return pl.pallas_call(
        mixing_kernel,
        in_specs=[pl.BlockSpec(memory_space=pltpu.SMEM)] + [whole] * 2,
        out_specs=[whole] * 2,
        out_shape=[jax.ShapeDtypeStruct((sent, rows), jnp.bfloat16)] * 2,
        compiler_params=pltpu.CompilerParams(vmem_limit_bytes=4 << 20),
        name="mixing",
    )(member.reshape(1), ids, scores)


def expert_kernel(x_hbm, *refs):
    gus, downs, out_hbm = refs[:GROUP], refs[GROUP : 2 * GROUP], refs[2 * GROUP]
    x_buf, gu_buf, down_buf, out_buf, x_sem, gu_sem, down_sem, out_sem = refs[2 * GROUP + 1 :]
    inner = downs[0].shape[0]
    width = out_hbm.shape[1]
    x_copy = pltpu.make_async_copy(x_hbm, x_buf, x_sem)
    gu_copies = [pltpu.make_async_copy(gus[s], gu_buf.at[s], gu_sem.at[s]) for s in range(GROUP)]
    down_copies = [
        pltpu.make_async_copy(downs[s], down_buf.at[pl.ds(s * inner, inner)], down_sem.at[s])
        for s in range(GROUP)
    ]
    x_copy.start()
    gu_copies[0].start()
    gu_copies[1].start()
    x_copy.wait()
    hidden = []
    for s in range(GROUP):
        gu_copies[s].wait()
        if s + 2 < GROUP:
            gu_copies[s + 2].start()
        down_copies[s].start()
        both = jnp.dot(x_buf[...], gu_buf[s], preferred_element_type=jnp.float32)
        g = jnp.minimum(both[:, :inner], clamp_limit)
        u = jnp.clip(both[:, inner:], -clamp_limit, clamp_limit)
        hidden.append(((u + 1.0) * g * jax.nn.sigmoid(swish_slope * g)).astype(jnp.bfloat16))
    hidden = jnp.concatenate(hidden, axis=1)
    for copy in down_copies:
        copy.wait()
    parts = out_sem.shape[0]
    step = width // parts
    out_copies = []
    for n in range(parts):
        own = pl.ds(n * step, step)
        out_buf[:, own] = jnp.dot(
            hidden, down_buf[:, own], preferred_element_type=jnp.float32
        ).astype(jnp.bfloat16)
        copy = pltpu.make_async_copy(out_buf.at[:, own], out_hbm.at[:, own], out_sem.at[n])
        copy.start()
        out_copies.append(copy)
    for copy in out_copies:
        copy.wait()


def expert(x, gus, downs):
    rows, width = x.shape
    inner = downs[0].shape[0]
    parts = 4
    outside = pl.BlockSpec(memory_space=pl.ANY)
    return pl.pallas_call(
        expert_kernel,
        in_specs=[outside] * (1 + 2 * GROUP),
        out_specs=outside,
        out_shape=jax.ShapeDtypeStruct((rows, width), jnp.bfloat16),
        scratch_shapes=[
            pltpu.VMEM((rows, width), jnp.bfloat16),
            pltpu.VMEM((GROUP, width, 2 * inner), jnp.bfloat16),
            pltpu.VMEM((GROUP * inner, width), jnp.bfloat16),
            pltpu.VMEM((rows, width), jnp.bfloat16),
            pltpu.SemaphoreType.DMA,
            pltpu.SemaphoreType.DMA((GROUP,)),
            pltpu.SemaphoreType.DMA((GROUP,)),
            pltpu.SemaphoreType.DMA((parts,)),
        ],
        compiler_params=pltpu.CompilerParams(vmem_limit_bytes=53000 << 10),
        name="expert",
    )(x, *gus, *downs)


def program(
    mixer_in,
    mixer_gain,
    w_value,
    w_gate,
    w_taps,
    channel_gain,
    w_output,
    expert_in,
    expert_gain,
    route_experts,
    route_scores,
    expert_gate,
    expert_up,
    expert_down,
):
    rows_b, width = expert_in.shape
    experts = lax.axis_size("ep")
    capacity = 2 * rows_b * TOP_K // experts
    slots = capacity // GROUP
    member = lax.axis_index(("y0", "c")).astype(jnp.int32)

    gate_up = jnp.concatenate([expert_gate[0], expert_up[0]], axis=1)
    down = expert_down[0]
    gu_y = swapped(gate_up, "y0")
    down_y = swapped(down, "y0")
    gu_c = swapped(gate_up, "c")
    down_c = swapped(down, "c")
    gu_d = swapped(gu_y, "c")
    down_d = swapped(down_y, "c")

    ids = route_experts.T
    sending = front(member, expert_in, expert_gain, ids, experts * slots)
    arrived = exchanged(sending.reshape(experts, slots, width), "ep").reshape(-1, width)

    mixing_hi, mixing_lo = mixing(member, ids, route_scores.T, experts * slots)
    conv_out = convolved(mixer_in, mixer_gain, w_value, w_gate, w_taps)
    mixer_partial = projected(conv_out, channel_gain, w_output)
    mixer_half = core_half(mixer_partial)

    partial = expert(arrived, (gate_up, gu_c, gu_y, gu_d), (down, down_c, down_y, down_d))
    returned = exchanged(partial.reshape(experts, slots, width), "ep").reshape(-1, width)

    def mixed(m):
        return lax.dot_general(
            m, returned, (((0,), (0,)), ((), ())), preferred_element_type=jnp.float32
        )

    expert_half = core_half(mixed(mixing_hi) + mixed(mixing_lo))
    mixer_out, expert_out = totals([mixer_half, expert_half])
    return (mixer_out, expert_out)


def solution(mesh):
    split = Mesh(mesh.devices.reshape(mesh.shape["ep"], 2, 2, 2, 2), ("ep", *TP))
    in_specs = (
        P("ep", None),
        P(),
        P(None, TP),
        P(None, TP),
        P(None, TP),
        P(TP),
        P(TP, None),
        P("ep", None),
        P(),
        P("ep", None),
        P("ep", None),
        P("ep", None, TP),
        P("ep", None, TP),
        P("ep", TP, None),
    )
    out_specs = (P("ep", None), P("ep", None))
    return jax.shard_map(program, mesh=split, in_specs=in_specs, out_specs=out_specs, check_vma=False)
```

profile of v0, /device:TPU:65, one launch (start us, length us, event | category | flops | bytes accessed | tf_op | source)
XLA Modules:
  0.0 161.2 jit_solution(18348185503552125259)
XLA Ops:
  0.6 0.0 copy-start
  0.7 2.4 %pad_maximum_fusion.refs_0_ = bf16[2048,256]{1,0:T(8,128)(2,1)} fusion(bf16[2048,128]{1,0:T(8,128)(2,1)} %bitcast.138, bf16[2048,128]{1,0:T(8,128)(2,1)} %bitcast.139), kind=kLoop, calls=%fused_computation.14 | loop fusion | flops 2097152 | bytes 2097152 | tf_op jit(solution)/shard_map/concatenate | solution.py:273
  3.0 3.2 %collective-permute-start.3 = (bf16[2048,256]{1,0:T(8,128)(2,1)}, bf16[2048,256]{1,0:T(8,128)(2,1)}, u32[]{:S(2)}, u32[]{:S(2)}) collective-permute-start(bf16[2048,256]{1,0:T(8,128)(2,1)} %pad_maximum_fusion.refs_0_), channel_id=1, source_target_pairs={{0,2},{2,0},{1,3},{3,1},{4,6},{6,4},{5,7},{7,5},{8,10},{10,8},{9,1... | collective-permute-start | bytes 3145736 | tf_op jit(solution)/shard_map/ppermute | solution.py:31
  6.3 1.8 %front.1 = bf16[256,2048]{1,0:T(8,128)(2,1)} custom-call(s32[1]{0:T(128)} %bitcast.40.member, bf16[128,2048]{1,0:T(8,128)(2,1)S(1)} %copy-done.1, f32[1,2048]{1,0:T(1,128)S(1)} %bitcast.129, s32[4,128]{1,0:T(4,128)S(1)} %bitcast.130), custom_call_target="tpu_custom_call" | custom-call | tf_op jit(solution)/shard_map/front/pallas_call | solution.py:141
  8.1 12.2 %all-to-all-start = ((bf16[32,8,2048]{2,1,0:T(8,128)(2,1)}), bf16[32,8,2048]{2,1,0:T(8,128)(2,1)}, u32[]{:S(2)}, u32[]{:S(2)}) async-start(bf16[32,8,2048]{2,1,0:T(8,128)(2,1)} %bitcast.44), calls=%async_computation | async-start | bytes 2097152 | tf_op jit(solution)/shard_map/all_to_all | solution.py:35
  20.3 2.1 %collective-permute-start.6 = (bf16[128,2048]{1,0:T(8,128)(2,1)S(1)}, bf16[128,2048]{1,0:T(8,128)(2,1)S(1)}, u32[]{:S(2)}, u32[]{:S(2)}) collective-permute-start(bf16[128,2048]{1,0:T(8,128)(2,1)S(1)} %bitcast.126), channel_id=1, source_target_pairs={{0,2},{2,0},{1,3},{3,1},{4,6},{6,4},{5,7},{7,5},{8,10},{10,8},{9,1... | collective-permute-start | bytes 1572872 | tf_op jit(solution)/shard_map/ppermute | solution.py:31
  22.4 3.7 %collective-permute-start.2 = (bf16[2048,256]{1,0:T(8,128)(2,1)}, bf16[2048,256]{1,0:T(8,128)(2,1)}, u32[]{:S(2)}, u32[]{:S(2)}) collective-permute-start(bf16[2048,256]{1,0:T(8,128)(2,1)} %pad_maximum_fusion.refs_0_), channel_id=1, source_target_pairs={{0,1},{1,0},{2,3},{3,2},{4,5},{5,4},{6,7},{7,6},{8,9},{9,8},{10,11... | collective-permute-start | bytes 3145736 | tf_op jit(solution)/shard_map/ppermute | solution.py:31
  26.1 3.2 %collective-permute-done.3.refs_2_ = bf16[2048,256]{1,0:T(8,128)(2,1)} collective-permute-done((bf16[2048,256]{1,0:T(8,128)(2,1)}, bf16[2048,256]{1,0:T(8,128)(2,1)}, u32[]{:S(2)}, u32[]{:S(2)}) %collective-permute-start.3) | collective-permute-done | bytes 1048608 | tf_op jit(solution)/shard_map/ppermute | solution.py:31
  29.3 4.6 %collective-permute-start.4 = (bf16[2048,256]{1,0:T(8,128)(2,1)}, bf16[2048,256]{1,0:T(8,128)(2,1)}, u32[]{:S(2)}, u32[]{:S(2)}) collective-permute-start(bf16[2048,256]{1,0:T(8,128)(2,1)} %collective-permute-done.3.refs_2_), channel_id=1, source_target_pairs={{0,1},{1,0},{2,3},{3,2},{4,5},{5,4},{6,7},{7,6},{8,9},{9,8},{10,11... | collective-permute-start | bytes 3145736 | tf_op jit(solution)/shard_map/ppermute | solution.py:31
  33.8 1.9 %collective-permute-start.5 = (bf16[128,2048]{1,0:T(8,128)(2,1)S(1)}, bf16[128,2048]{1,0:T(8,128)(2,1)S(1)}, u32[]{:S(2)}, u32[]{:S(2)}) collective-permute-start(bf16[128,2048]{1,0:T(8,128)(2,1)S(1)} %bitcast.127), channel_id=1, source_target_pairs={{0,1},{1,0},{2,3},{3,2},{4,5},{5,4},{6,7},{7,6},{8,9},{9,8},{10,11... | collective-permute-start | bytes 1572872 | tf_op jit(solution)/shard_map/ppermute | solution.py:31
  35.8 0.2 convert_reduce_fusion
  35.9 4.6 %collective-permute-done.6.refs_6_ = bf16[128,2048]{1,0:T(8,128)(2,1)S(1)} collective-permute-done((bf16[128,2048]{1,0:T(8,128)(2,1)S(1)}, bf16[128,2048]{1,0:T(8,128)(2,1)S(1)}, u32[]{:S(2)}, u32[]{:S(2)}) %collective-permute-start.6) | collective-permute-done | bytes 524320 | tf_op jit(solution)/shard_map/ppermute | solution.py:31
  40.5 3.3 %collective-permute-start.7 = (bf16[128,2048]{1,0:T(8,128)(2,1)S(1)}, bf16[128,2048]{1,0:T(8,128)(2,1)S(1)}, u32[]{:S(2)}, u32[]{:S(2)}) collective-permute-start(bf16[128,2048]{1,0:T(8,128)(2,1)S(1)} %collective-permute-done.6.refs_6_), channel_id=1, source_target_pairs={{0,1},{1,0},{2,3},{3,2},{4,5},{5,4},{6,7},{7,6},{8,9},{9,8},{10,11... | collective-permute-start | bytes 1572872 | tf_op jit(solution)/shard_map/ppermute | solution.py:31
  43.9 0.3 fusion.7
  44.2 0.0 collective-permute-done.5.refs_5_
  44.2 1.2 collective-permute-done.7.refs_7_
  45.4 0.0 collective-permute-done.2.refs_1_
  45.4 0.3 all-to-all-done
  45.7 6.1 %expert.1 = bf16[256,2048]{1,0:T(8,128)(2,1)} custom-call(bf16[256,2048]{1,0:T(8,128)(2,1)} %bitcast.45.x_hbm, bf16[2048,256]{1,0:T(8,128)(2,1)} %pad_maximum_fusion.refs_0_, bf16[2048,256]{1,0:T(8,128)(2,1)} %collective-permute-done.2.refs_1_, bf16[2048,256]{1,0:T(8,128)(2,1)} %collective-permute-done.3.refs_2_, ...), custom_call_target="tpu_custom_call" | custom-call | tf_op jit(solution)/shard_map/expert/pallas_call | solution.py:231
  51.8 0.0 copy-start.9
  51.8 0.0 copy-start.11
  51.8 11.9 %all-to-all-start.1 = ((bf16[32,8,2048]{2,1,0:T(8,128)(2,1)}), bf16[32,8,2048]{2,1,0:T(8,128)(2,1)S(1)}, u32[]{:S(2)}, u32[]{:S(2)}) async-start(bf16[32,8,2048]{2,1,0:T(8,128)(2,1)} %bitcast.133), calls=%async_computation.1 | async-start | bytes 2097152 | tf_op jit(solution)/shard_map/all_to_all | solution.py:35
  63.7 0.0 copy-start.10
  63.7 0.4 fusion.57
  64.1 0.6 copy-done.10
  64.7 0.4 fusion.6
  65.1 0.1 slice.272
  65.2 3.1 %collective-permute-start = (bf16[30,96]{0,1:T(8,128)(2,1)S(1)}, bf16[30,96]{0,1:T(8,128)(2,1)S(1)}, u32[]{:S(2)}, u32[]{:S(2)}) collective-permute-start(bf16[30,96]{0,1:T(8,128)(2,1)S(1)} %slice.272), channel_id=1, source_target_pairs={{0,16},{16,32},{32,48},{48,64},{64,80},{80,96},{96,112},{112,128},... | collective-permute-start | bytes 17288 | tf_op jit(solution)/shard_map/ppermute | solution.py:27
  68.3 0.3 mixing.1
  68.7 19.1 %collective-permute-done = bf16[30,96]{0,1:T(8,128)(2,1)S(1)} collective-permute-done((bf16[30,96]{0,1:T(8,128)(2,1)S(1)}, bf16[30,96]{0,1:T(8,128)(2,1)S(1)}, u32[]{:S(2)}, u32[]{:S(2)}) %collective-permute-start) | collective-permute-done | bytes 5792 | tf_op jit(solution)/shard_map/ppermute | solution.py:27
  87.7 0.9 fusion.59
  88.6 19.5 %all-gather.1 = f32[16,2,128]{2,1,0:T(2,128)S(1)} all-gather(f32[1,2,128]{2,1,0:T(2,128)S(1)} %maximum_bitcast_fusion), channel_id=2, replica_groups=mesh['ep'=32,'y2'=2,'y1'=2,'y0'=2,'c'=2] {'y2','y1','y0','c'}, dimensions={0}, use_global_device_ids=true | all-gather | bytes 17408 | tf_op jit(solution)/shard_map/all_gather | solution.py:92
  108.2 0.4 fusion.19
  108.6 2.1 %collective-permute-start.1 = (bf16[64,2048]{1,0:T(8,128)(2,1)S(1)}, bf16[64,2048]{1,0:T(8,128)(2,1)S(1)}, u32[]{:S(2)}, u32[]{:S(2)}) collective-permute-start(bf16[64,2048]{1,0:T(8,128)(2,1)S(1)} %fusion.15), channel_id=1, source_target_pairs={{0,1},{1,0},{2,3},{3,2},{4,5},{5,4},{6,7},{7,6},{8,9},{9,8},{10,11... | collective-permute-start | bytes 786440 | tf_op jit(solution)/shard_map/ppermute | solution.py:31
  110.7 0.3 fusion.10
  111.1 0.3 convolution_add_fusion
  111.5 2.2 %collective-permute-start.8 = (bf16[64,2048]{1,0:T(8,128)(2,1)S(1)}, bf16[64,2048]{1,0:T(8,128)(2,1)S(1)}, u32[]{:S(2)}, u32[]{:S(2)}) collective-permute-start(bf16[64,2048]{1,0:T(8,128)(2,1)S(1)} %fusion.16), channel_id=1, source_target_pairs={{0,1},{1,0},{2,3},{3,2},{4,5},{5,4},{6,7},{7,6},{8,9},{9,8},{10,11... | collective-permute-start | bytes 786440 | tf_op jit(solution)/shard_map/ppermute | solution.py:31
  113.7 0.1 fusion.17
  113.8 1.1 collective-permute-done.8
  114.9 0.1 fusion.18
  115.0 0.1 pad_maximum_fusion.1
  115.0 20.7 %all_to_all.20 = bf16[8,2,8,2048]{3,2,1,0:T(8,128)(2,1)S(1)} all-to-all(bf16[8,2,8,2048]{3,2,1,0:T(8,128)(2,1)S(1)} %pad_maximum_fusion.1), channel_id=1, replica_groups=mesh['ep'=32,'y2'=2,'y1'=2,'y0'=2,'c'=2] {'y2','y1','y0'}, dimensions={0} | all-to-all | bytes 1048576 | tf_op jit(solution)/shard_map/all_to_all | solution.py:35
  135.7 0.1 reduce_sum.62
  135.8 17.7 %all_to_all.21 = bf16[8,2,8,2048]{3,2,1,0:T(8,128)(2,1)S(1)} all-to-all(bf16[8,2,8,2048]{3,2,1,0:T(8,128)(2,1)S(1)} %broadcast_in_dim.2), channel_id=1, replica_groups=mesh['ep'=32,'y2'=2,'y1'=2,'y0'=2,'c'=2] {'y2','y1','y0'}, dimensions={0} | all-to-all | bytes 1048576 | tf_op jit(solution)/shard_map/all_to_all | solution.py:35
  153.5 5.1 %collective-permute-start.9 = (bf16[8,2,8,2048]{3,2,1,0:T(8,128)(2,1)S(1)}, bf16[8,2,8,2048]{3,2,1,0:T(8,128)(2,1)S(1)}, u32[]{:S(2)}, u32[]{:S(2)}) collective-permute-start(bf16[8,2,8,2048]{3,2,1,0:T(8,128)(2,1)S(1)} %all_to_all.21), channel_id=1, source_target_pairs={{0,1},{1,0},{2,3},{3,2},{4,5},{5,4},{6,7},{7,6},{8,9},{9,8},{10,11... | collective-permute-start | bytes 1572872 | tf_op jit(solution)/shard_map/ppermute | solution.py:31
  158.6 1.5 collective-permute-done.9
  160.1 0.1 select_bitcast_fusion.1
  160.2 1.0 pad_maximum_fusion.2
  (33 shorter events, 0.3 us)
Async XLA Ops:
  0.6 107.5 %copy-start = (bf16[96,2048]{1,0:T(8,128)(2,1)S(1)}, bf16[96,2048]{1,0:T(8,128)(2,1)}, u32[]{:S(2)}) copy-start(bf16[96,2048]{1,0:T(8,128)(2,1)} %param.20) | copy-start | bytes 1179652
  0.6 5.6 %copy-start.1 = (bf16[128,2048]{1,0:T(8,128)(2,1)S(1)}, bf16[128,2048]{1,0:T(8,128)(2,1)}, u32[]{:S(2)}) copy-start(bf16[128,2048]{1,0:T(8,128)(2,1)} %x_ref.1) | copy-start | bytes 1572868
  0.7 5.6 %copy-start.3 = (f32[2048]{0:T(1024)S(1)}, f32[2048]{0:T(1024)}, u32[]{:S(2)}) copy-start(f32[2048]{0:T(1024)} %param.22) | copy-start | bytes 24580
  0.7 5.6 %copy-start.4 = (s32[128,4]{0,1:T(4,128)S(1)}, s32[128,4]{0,1:T(4,128)}, u32[]{:S(2)}) copy-start(s32[128,4]{0,1:T(4,128)} %param.23) | copy-start | bytes 6148
  3.0 26.2 %collective-permute-start.3 = (bf16[2048,256]{1,0:T(8,128)(2,1)}, bf16[2048,256]{1,0:T(8,128)(2,1)}, u32[]{:S(2)}, u32[]{:S(2)}) collective-permute-start(bf16[2048,256]{1,0:T(8,128)(2,1)} %pad_maximum_fusion.refs_0_), channel_id=1, source_target_pairs={{0,2},{2,0},{1,3},{3,1},{4,6},{6,4},{5,7},{7,5},{8,10},{10,8},{9,1... | collective-permute-start | bytes 3145736 | tf_op jit(solution)/shard_map/ppermute | solution.py:31
  8.1 12.2 %copy-start.2 = (bf16[1,128,2048]{2,1,0:T(8,128)(2,1)S(1)}, bf16[1,128,2048]{2,1,0:T(8,128)(2,1)}, u32[]{:S(2)}) copy-start(bf16[1,128,2048]{2,1,0:T(8,128)(2,1)} %param.27) | copy-start | bytes 1572868
  8.1 27.7 %copy-start.6 = (bf16[128,2048]{1,0:T(8,128)(2,1)S(1)}, bf16[128,2048]{1,0:T(8,128)(2,1)}, u32[]{:S(2)}) copy-start(bf16[128,2048]{1,0:T(8,128)(2,1)} %param.14) | copy-start | bytes 1572868
  8.1 37.6 %all-to-all-start = ((bf16[32,8,2048]{2,1,0:T(8,128)(2,1)}), bf16[32,8,2048]{2,1,0:T(8,128)(2,1)}, u32[]{:S(2)}, u32[]{:S(2)}) async-start(bf16[32,8,2048]{2,1,0:T(8,128)(2,1)} %bitcast.44), calls=%async_computation | async-start | bytes 2097152 | tf_op jit(solution)/shard_map/all_to_all | solution.py:35
  20.3 20.2 %collective-permute-start.6 = (bf16[128,2048]{1,0:T(8,128)(2,1)S(1)}, bf16[128,2048]{1,0:T(8,128)(2,1)S(1)}, u32[]{:S(2)}, u32[]{:S(2)}) collective-permute-start(bf16[128,2048]{1,0:T(8,128)(2,1)S(1)} %bitcast.126), channel_id=1, source_target_pairs={{0,2},{2,0},{1,3},{3,1},{4,6},{6,4},{5,7},{7,5},{8,10},{10,8},{9,1... | collective-permute-start | bytes 1572872 | tf_op jit(solution)/shard_map/ppermute | solution.py:31
  22.4 23.0 %collective-permute-start.2 = (bf16[2048,256]{1,0:T(8,128)(2,1)}, bf16[2048,256]{1,0:T(8,128)(2,1)}, u32[]{:S(2)}, u32[]{:S(2)}) collective-permute-start(bf16[2048,256]{1,0:T(8,128)(2,1)} %pad_maximum_fusion.refs_0_), channel_id=1, source_target_pairs={{0,1},{1,0},{2,3},{3,2},{4,5},{5,4},{6,7},{7,6},{8,9},{9,8},{10,11... | collective-permute-start | bytes 3145736 | tf_op jit(solution)/shard_map/ppermute | solution.py:31
  29.3 16.4 %collective-permute-start.4 = (bf16[2048,256]{1,0:T(8,128)(2,1)}, bf16[2048,256]{1,0:T(8,128)(2,1)}, u32[]{:S(2)}, u32[]{:S(2)}) collective-permute-start(bf16[2048,256]{1,0:T(8,128)(2,1)} %collective-permute-done.3.refs_2_), channel_id=1, source_target_pairs={{0,1},{1,0},{2,3},{3,2},{4,5},{5,4},{6,7},{7,6},{8,9},{9,8},{10,11... | collective-permute-start | bytes 3145736 | tf_op jit(solution)/shard_map/ppermute | solution.py:31
  33.8 10.3 %collective-permute-start.5 = (bf16[128,2048]{1,0:T(8,128)(2,1)S(1)}, bf16[128,2048]{1,0:T(8,128)(2,1)S(1)}, u32[]{:S(2)}, u32[]{:S(2)}) collective-permute-start(bf16[128,2048]{1,0:T(8,128)(2,1)S(1)} %bitcast.127), channel_id=1, source_target_pairs={{0,1},{1,0},{2,3},{3,2},{4,5},{5,4},{6,7},{7,6},{8,9},{9,8},{10,11... | collective-permute-start | bytes 1572872 | tf_op jit(solution)/shard_map/ppermute | solution.py:31
  40.5 4.8 %collective-permute-start.7 = (bf16[128,2048]{1,0:T(8,128)(2,1)S(1)}, bf16[128,2048]{1,0:T(8,128)(2,1)S(1)}, u32[]{:S(2)}, u32[]{:S(2)}) collective-permute-start(bf16[128,2048]{1,0:T(8,128)(2,1)S(1)} %collective-permute-done.6.refs_6_), channel_id=1, source_target_pairs={{0,1},{1,0},{2,3},{3,2},{4,5},{5,4},{6,7},{7,6},{8,9},{9,8},{10,11... | collective-permute-start | bytes 1572872 | tf_op jit(solution)/shard_map/ppermute | solution.py:31
  51.8 11.9 %copy-start.9 = (bf16[2048,96]{0,1:T(8,128)(2,1)S(1)}, bf16[2048,96]{0,1:T(8,128)(2,1)}, u32[]{:S(2)}) copy-start(bf16[2048,96]{0,1:T(8,128)(2,1)} %param.16) | copy-start | bytes 1179652
  51.8 11.9 %copy-start.11 = (f32[2048]{0:T(1024)S(1)}, f32[2048]{0:T(1024)}, u32[]{:S(2)}) copy-start(f32[2048]{0:T(1024)} %param.15) | copy-start | bytes 24580
  51.8 59.0 %all-to-all-start.1 = ((bf16[32,8,2048]{2,1,0:T(8,128)(2,1)}), bf16[32,8,2048]{2,1,0:T(8,128)(2,1)S(1)}, u32[]{:S(2)}, u32[]{:S(2)}) async-start(bf16[32,8,2048]{2,1,0:T(8,128)(2,1)} %bitcast.133), calls=%async_computation.1 | async-start | bytes 2097152 | tf_op jit(solution)/shard_map/all_to_all | solution.py:35
  63.7 1.0 copy-start.10
  64.7 3.6 %copy-start.7 = (f32[31,96]{1,0:T(8,128)S(1)}, f32[31,96]{1,0:T(8,128)}, u32[]{:S(2)}) copy-start(f32[31,96]{1,0:T(8,128)} %param.18) | copy-start | bytes 35716
  64.7 3.7 %copy-start.5 = (f32[128,4]{0,1:T(4,128)S(1)}, f32[128,4]{0,1:T(4,128)}, u32[]{:S(2)}) copy-start(f32[128,4]{0,1:T(4,128)} %param.24) | copy-start | bytes 6148
  64.7 43.5 %copy-start.8 = (f32[96]{0:T(128)S(1)}, f32[96]{0:T(128)}, u32[]{:S(2)}) copy-start(f32[96]{0:T(128)} %param.19) | copy-start | bytes 1156
  65.2 22.6 %collective-permute-start = (bf16[30,96]{0,1:T(8,128)(2,1)S(1)}, bf16[30,96]{0,1:T(8,128)(2,1)S(1)}, u32[]{:S(2)}, u32[]{:S(2)}) collective-permute-start(bf16[30,96]{0,1:T(8,128)(2,1)S(1)} %slice.272), channel_id=1, source_target_pairs={{0,16},{16,32},{32,48},{48,64},{64,80},{80,96},{96,112},{112,128},... | collective-permute-start | bytes 17288 | tf_op jit(solution)/shard_map/ppermute | solution.py:27
  108.6 5.1 %collective-permute-start.1 = (bf16[64,2048]{1,0:T(8,128)(2,1)S(1)}, bf16[64,2048]{1,0:T(8,128)(2,1)S(1)}, u32[]{:S(2)}, u32[]{:S(2)}) collective-permute-start(bf16[64,2048]{1,0:T(8,128)(2,1)S(1)} %fusion.15), channel_id=1, source_target_pairs={{0,1},{1,0},{2,3},{3,2},{4,5},{5,4},{6,7},{7,6},{8,9},{9,8},{10,11... | collective-permute-start | bytes 786440 | tf_op jit(solution)/shard_map/ppermute | solution.py:31
  111.5 3.4 %collective-permute-start.8 = (bf16[64,2048]{1,0:T(8,128)(2,1)S(1)}, bf16[64,2048]{1,0:T(8,128)(2,1)S(1)}, u32[]{:S(2)}, u32[]{:S(2)}) collective-permute-start(bf16[64,2048]{1,0:T(8,128)(2,1)S(1)} %fusion.16), channel_id=1, source_target_pairs={{0,1},{1,0},{2,3},{3,2},{4,5},{5,4},{6,7},{7,6},{8,9},{9,8},{10,11... | collective-permute-start | bytes 786440 | tf_op jit(solution)/shard_map/ppermute | solution.py:31
  153.5 6.6 %collective-permute-start.9 = (bf16[8,2,8,2048]{3,2,1,0:T(8,128)(2,1)S(1)}, bf16[8,2,8,2048]{3,2,1,0:T(8,128)(2,1)S(1)}, u32[]{:S(2)}, u32[]{:S(2)}) collective-permute-start(bf16[8,2,8,2048]{3,2,1,0:T(8,128)(2,1)S(1)} %all_to_all.21), channel_id=1, source_target_pairs={{0,1},{1,0},{2,3},{3,2},{4,5},{5,4},{6,7},{7,6},{8,9},{9,8},{10,11... | collective-permute-start | bytes 1572872 | tf_op jit(solution)/shard_map/ppermute | solution.py:31
where the time goes:
time: 162 us; the launch traced here: 161 us
  blocking collectives  57.9 us (36%)
  starting transfers between devices  55.3 us (34%)
  waiting for transfers between devices  31 us (19%)
  Pallas kernels  8.18 us (5%)
  other arithmetic  5.06 us (3%)
  matrix products  1.9 us (1%)
    all_to_all x2, blocking collectives, exchanged(): return lax.all_to_all(x, axis, split_axis=0, concat_axis=0, tiled=True)  38.4 us
    ppermute x9, starting transfers between devices, swapped(): return lax.ppermute(x, axis, [(0, 1), (1, 0)])  28.2 us
    all_to_all x2, starting transfers between devices, exchanged(): return lax.all_to_all(x, axis, split_axis=0, concat_axis=0, tiled=True)  24.1 us
    all_gather x1, blocking collectives, projected(): everyone = lax.all_gather(sums, TP)  19.5 us
    ppermute x1, waiting for transfers between devices, shifted(): return lax.ppermute(block, axis, route)  19.1 us
    ppermute x9, waiting for transfers between devices, swapped(): return lax.ppermute(x, axis, [(0, 1), (1, 0)])  11.6 us
    pallas_call x1, Pallas kernels, expert(): pl.pallas_call(expert_kernel, in_specs=[outside] * (1 + 2 * GROUP), out_s...  6.06 us
  transfers between devices with their start and end apart: 12, of which 7 were waited for; matrix products, arithmetic and copies ran while one was open for 2% of the time, Pallas kernels for 1%

commit v1 on v0

--- a/solution.py
+++ b/solution.py
@@ -180,69 +180,32 @@
     )(member.reshape(1), ids, scores)
 
 
-def expert_kernel(x_hbm, *refs):
-    gus, downs, out_hbm = refs[:GROUP], refs[GROUP : 2 * GROUP], refs[2 * GROUP]
-    x_buf, gu_buf, down_buf, out_buf, x_sem, gu_sem, down_sem, out_sem = refs[2 * GROUP + 1 :]
+def expert_kernel(x_ref, *refs):
+    gus, downs, out_ref = refs[:GROUP], refs[GROUP : 2 * GROUP], refs[2 * GROUP]
     inner = downs[0].shape[0]
-    width = out_hbm.shape[1]
-    x_copy = pltpu.make_async_copy(x_hbm, x_buf, x_sem)
-    gu_copies = [pltpu.make_async_copy(gus[s], gu_buf.at[s], gu_sem.at[s]) for s in range(GROUP)]
-    down_copies = [
-        pltpu.make_async_copy(downs[s], down_buf.at[pl.ds(s * inner, inner)], down_sem.at[s])
-        for s in range(GROUP)
-    ]
-    x_copy.start()
-    gu_copies[0].start()
-    gu_copies[1].start()
-    x_copy.wait()
+    width = out_ref.shape[1]
     hidden = []
-    for s in range(GROUP):
-        gu_copies[s].wait()
-        if s + 2 < GROUP:
-            gu_copies[s + 2].start()
-        down_copies[s].start()
-        both = jnp.dot(x_buf[...], gu_buf[s], preferred_element_type=jnp.float32)
+    for gu in gus:
+        both = jnp.dot(x_ref[...], gu[...], preferred_element_type=jnp.float32)
         g = jnp.minimum(both[:, :inner], clamp_limit)
         u = jnp.clip(both[:, inner:], -clamp_limit, clamp_limit)
         hidden.append(((u + 1.0) * g * jax.nn.sigmoid(swish_slope * g)).astype(jnp.bfloat16))
     hidden = jnp.concatenate(hidden, axis=1)
-    for copy in down_copies:
-        copy.wait()
-    parts = out_sem.shape[0]
-    step = width // parts
-    out_copies = []
-    for n in range(parts):
-        own = pl.ds(n * step, step)
-        out_buf[:, own] = jnp.dot(
-            hidden, down_buf[:, own], preferred_element_type=jnp.float32
+    step = 512
+    for at in range(0, width, step):
+        weights = jnp.concatenate([down[:, at : at + step] for down in downs], axis=0)
+        out_ref[:, at : at + step] = jnp.dot(
+            hidden, weights, preferred_element_type=jnp.float32
         ).astype(jnp.bfloat16)
-        copy = pltpu.make_async_copy(out_buf.at[:, own], out_hbm.at[:, own], out_sem.at[n])
-        copy.start()
-        out_copies.append(copy)
-    for copy in out_copies:
-        copy.wait()
 
 
 def expert(x, gus, downs):
-    rows, width = x.shape
-    inner = downs[0].shape[0]
-    parts = 4
-    outside = pl.BlockSpec(memory_space=pl.ANY)
+    whole = pl.BlockSpec(memory_space=pltpu.VMEM)
     return pl.pallas_call(
         expert_kernel,
-        in_specs=[outside] * (1 + 2 * GROUP),
-        out_specs=outside,
-        out_shape=jax.ShapeDtypeStruct((rows, width), jnp.bfloat16),
-        scratch_shapes=[
-            pltpu.VMEM((rows, width), jnp.bfloat16),
-            pltpu.VMEM((GROUP, width, 2 * inner), jnp.bfloat16),
-            pltpu.VMEM((GROUP * inner, width), jnp.bfloat16),
-            pltpu.VMEM((rows, width), jnp.bfloat16),
-            pltpu.SemaphoreType.DMA,
-            pltpu.SemaphoreType.DMA((GROUP,)),
-            pltpu.SemaphoreType.DMA((GROUP,)),
-            pltpu.SemaphoreType.DMA((parts,)),
-        ],
+        in_specs=[whole] * (1 + 2 * GROUP),
+        out_specs=whole,
+        out_shape=jax.ShapeDtypeStruct(x.shape, jnp.bfloat16),
         compiler_params=pltpu.CompilerParams(vmem_limit_bytes=53000 << 10),
         name="expert",
     )(x, *gus, *downs)

time: 162 us -> 161 us (level)
  no operation moved by 1% of the time
where the time goes in v1:
time: 161 us; the launch traced here: 160 us
  blocking collectives  57.9 us (36%)
  starting transfers between devices  55.3 us (34%)
  waiting for transfers between devices  31 us (19%)
  Pallas kernels  7.41 us (5%)
  other arithmetic  5.06 us (3%)
  matrix products  1.9 us (1%)
    all_to_all x2, blocking collectives, exchanged(): return lax.all_to_all(x, axis, split_axis=0, concat_axis=0, tiled=True)  38.4 us
    ppermute x9, starting transfers between devices, swapped(): return lax.ppermute(x, axis, [(0, 1), (1, 0)])  28.1 us
    all_to_all x2, starting transfers between devices, exchanged(): return lax.all_to_all(x, axis, split_axis=0, concat_axis=0, tiled=True)  24.1 us
    all_gather x1, blocking collectives, projected(): everyone = lax.all_gather(sums, TP)  19.5 us
    ppermute x1, waiting for transfers between devices, shifted(): return lax.ppermute(block, axis, route)  19.1 us
    ppermute x9, waiting for transfers between devices, swapped(): return lax.ppermute(x, axis, [(0, 1), (1, 0)])  11.6 us
    pallas_call x1, Pallas kernels, expert(): pl.pallas_call(expert_kernel, in_specs=[whole] * (1 + 2 * GROUP), out_spe...  5.29 us
  transfers between devices with their start and end apart: 12, of which 7 were waited for; matrix products, arithmetic and copies ran while one was open for 2% of the time, Pallas kernels for 1%

profile of v1, /device:TPU:65, one launch (start us, length us, event | category | flops | bytes accessed | tf_op | source)
XLA Modules:
  0.0 160.4 jit_solution(14331615150774661124)
XLA Ops:
  0.6 0.0 copy-start
  0.7 2.4 %pad_maximum_fusion.refs_0_ = bf16[2048,256]{1,0:T(8,128)(2,1)} fusion(bf16[2048,128]{1,0:T(8,128)(2,1)} %bitcast.138, bf16[2048,128]{1,0:T(8,128)(2,1)} %bitcast.139), kind=kLoop, calls=%fused_computation.14 | loop fusion | flops 2097152 | bytes 2097152 | tf_op jit(solution)/shard_map/concatenate | solution.py:236
  3.0 3.2 %collective-permute-start.3 = (bf16[2048,256]{1,0:T(8,128)(2,1)}, bf16[2048,256]{1,0:T(8,128)(2,1)}, u32[]{:S(2)}, u32[]{:S(2)}) collective-permute-start(bf16[2048,256]{1,0:T(8,128)(2,1)} %pad_maximum_fusion.refs_0_), channel_id=1, source_target_pairs={{0,2},{2,0},{1,3},{3,1},{4,6},{6,4},{5,7},{7,5},{8,10},{10,8},{9,1... | collective-permute-start | bytes 3145736 | tf_op jit(solution)/shard_map/ppermute | solution.py:31
  6.3 1.8 %front.1 = bf16[256,2048]{1,0:T(8,128)(2,1)} custom-call(s32[1]{0:T(128)} %bitcast.40.member, bf16[128,2048]{1,0:T(8,128)(2,1)S(1)} %copy-done.1, f32[1,2048]{1,0:T(1,128)S(1)} %bitcast.129, s32[4,128]{1,0:T(4,128)S(1)} %bitcast.130), custom_call_target="tpu_custom_call" | custom-call | tf_op jit(solution)/shard_map/front/pallas_call | solution.py:141
  8.1 12.2 %all-to-all-start = ((bf16[32,8,2048]{2,1,0:T(8,128)(2,1)}), bf16[32,8,2048]{2,1,0:T(8,128)(2,1)}, u32[]{:S(2)}, u32[]{:S(2)}) async-start(bf16[32,8,2048]{2,1,0:T(8,128)(2,1)} %bitcast.44), calls=%async_computation | async-start | bytes 2097152 | tf_op jit(solution)/shard_map/all_to_all | solution.py:35
  20.3 2.1 %collective-permute-start.6 = (bf16[128,2048]{1,0:T(8,128)(2,1)S(1)}, bf16[128,2048]{1,0:T(8,128)(2,1)S(1)}, u32[]{:S(2)}, u32[]{:S(2)}) collective-permute-start(bf16[128,2048]{1,0:T(8,128)(2,1)S(1)} %bitcast.126), channel_id=1, source_target_pairs={{0,2},{2,0},{1,3},{3,1},{4,6},{6,4},{5,7},{7,5},{8,10},{10,8},{9,1... | collective-permute-start | bytes 1572872 | tf_op jit(solution)/shard_map/ppermute | solution.py:31
  22.4 3.7 %collective-permute-start.2 = (bf16[2048,256]{1,0:T(8,128)(2,1)}, bf16[2048,256]{1,0:T(8,128)(2,1)}, u32[]{:S(2)}, u32[]{:S(2)}) collective-permute-start(bf16[2048,256]{1,0:T(8,128)(2,1)} %pad_maximum_fusion.refs_0_), channel_id=1, source_target_pairs={{0,1},{1,0},{2,3},{3,2},{4,5},{5,4},{6,7},{7,6},{8,9},{9,8},{10,11... | collective-permute-start | bytes 3145736 | tf_op jit(solution)/shard_map/ppermute | solution.py:31
  26.1 3.2 %collective-permute-done.3.refs_2_ = bf16[2048,256]{1,0:T(8,128)(2,1)} collective-permute-done((bf16[2048,256]{1,0:T(8,128)(2,1)}, bf16[2048,256]{1,0:T(8,128)(2,1)}, u32[]{:S(2)}, u32[]{:S(2)}) %collective-permute-start.3) | collective-permute-done | bytes 1048608 | tf_op jit(solution)/shard_map/ppermute | solution.py:31
  29.3 4.6 %collective-permute-start.4 = (bf16[2048,256]{1,0:T(8,128)(2,1)}, bf16[2048,256]{1,0:T(8,128)(2,1)}, u32[]{:S(2)}, u32[]{:S(2)}) collective-permute-start(bf16[2048,256]{1,0:T(8,128)(2,1)} %collective-permute-done.3.refs_2_), channel_id=1, source_target_pairs={{0,1},{1,0},{2,3},{3,2},{4,5},{5,4},{6,7},{7,6},{8,9},{9,8},{10,11... | collective-permute-start | bytes 3145736 | tf_op jit(solution)/shard_map/ppermute | solution.py:31
  33.8 1.9 %collective-permute-start.5 = (bf16[128,2048]{1,0:T(8,128)(2,1)S(1)}, bf16[128,2048]{1,0:T(8,128)(2,1)S(1)}, u32[]{:S(2)}, u32[]{:S(2)}) collective-permute-start(bf16[128,2048]{1,0:T(8,128)(2,1)S(1)} %bitcast.127), channel_id=1, source_target_pairs={{0,1},{1,0},{2,3},{3,2},{4,5},{5,4},{6,7},{7,6},{8,9},{9,8},{10,11... | collective-permute-start | bytes 1572872 | tf_op jit(solution)/shard_map/ppermute | solution.py:31
  35.8 0.2 convert_reduce_fusion
  35.9 4.6 %collective-permute-done.6.refs_6_ = bf16[128,2048]{1,0:T(8,128)(2,1)S(1)} collective-permute-done((bf16[128,2048]{1,0:T(8,128)(2,1)S(1)}, bf16[128,2048]{1,0:T(8,128)(2,1)S(1)}, u32[]{:S(2)}, u32[]{:S(2)}) %collective-permute-start.6) | collective-permute-done | bytes 524320 | tf_op jit(solution)/shard_map/ppermute | solution.py:31
  40.5 3.3 %collective-permute-start.7 = (bf16[128,2048]{1,0:T(8,128)(2,1)S(1)}, bf16[128,2048]{1,0:T(8,128)(2,1)S(1)}, u32[]{:S(2)}, u32[]{:S(2)}) collective-permute-start(bf16[128,2048]{1,0:T(8,128)(2,1)S(1)} %collective-permute-done.6.refs_6_), channel_id=1, source_target_pairs={{0,1},{1,0},{2,3},{3,2},{4,5},{5,4},{6,7},{7,6},{8,9},{9,8},{10,11... | collective-permute-start | bytes 1572872 | tf_op jit(solution)/shard_map/ppermute | solution.py:31
  43.9 0.3 fusion.7
  44.2 0.0 collective-permute-done.5.refs_5_
  44.2 1.2 collective-permute-done.7.refs_7_
  45.4 0.0 collective-permute-done.2.refs_1_
  45.4 0.3 all-to-all-done
  45.7 0.0 collective-permute-done.4.refs_3_
  45.7 5.3 %expert.1 = bf16[256,2048]{1,0:T(8,128)(2,1)} custom-call(bf16[256,2048]{1,0:T(8,128)(2,1)} %bitcast.45.x_ref, bf16[2048,256]{1,0:T(8,128)(2,1)} %pad_maximum_fusion.refs_0_, bf16[2048,256]{1,0:T(8,128)(2,1)} %collective-permute-done.2.refs_1_, bf16[2048,256]{1,0:T(8,128)(2,1)} %collective-permute-done.3.refs_2_, ...), custom_call_target="tpu_custom_call" | custom-call | tf_op jit(solution)/shard_map/expert/pallas_call | solution.py:204
  51.0 11.8 %all-to-all-start.1 = ((bf16[32,8,2048]{2,1,0:T(8,128)(2,1)}), bf16[32,8,2048]{2,1,0:T(8,128)(2,1)S(1)}, u32[]{:S(2)}, u32[]{:S(2)}) async-start(bf16[32,8,2048]{2,1,0:T(8,128)(2,1)} %bitcast.133), calls=%async_computation.1 | async-start | bytes 2097152 | tf_op jit(solution)/shard_map/all_to_all | solution.py:35
  62.9 0.0 copy-start.10
  62.9 0.4 fusion.57
  63.3 0.6 copy-done.10
  63.9 0.4 fusion.6
  64.3 0.1 slice.272
  64.4 3.1 %collective-permute-start = (bf16[30,96]{0,1:T(8,128)(2,1)S(1)}, bf16[30,96]{0,1:T(8,128)(2,1)S(1)}, u32[]{:S(2)}, u32[]{:S(2)}) collective-permute-start(bf16[30,96]{0,1:T(8,128)(2,1)S(1)} %slice.272), channel_id=1, source_target_pairs={{0,16},{16,32},{32,48},{48,64},{64,80},{80,96},{96,112},{112,128},... | collective-permute-start | bytes 17288 | tf_op jit(solution)/shard_map/ppermute | solution.py:27
  67.5 0.3 mixing.1
  67.8 19.1 %collective-permute-done = bf16[30,96]{0,1:T(8,128)(2,1)S(1)} collective-permute-done((bf16[30,96]{0,1:T(8,128)(2,1)S(1)}, bf16[30,96]{0,1:T(8,128)(2,1)S(1)}, u32[]{:S(2)}, u32[]{:S(2)}) %collective-permute-start) | collective-permute-done | bytes 5792 | tf_op jit(solution)/shard_map/ppermute | solution.py:27
  86.9 0.9 fusion.59
  87.8 19.5 %all-gather.1 = f32[16,2,128]{2,1,0:T(2,128)S(1)} all-gather(f32[1,2,128]{2,1,0:T(2,128)S(1)} %maximum_bitcast_fusion), channel_id=2, replica_groups=mesh['ep'=32,'y2'=2,'y1'=2,'y0'=2,'c'=2] {'y2','y1','y0','c'}, dimensions={0}, use_global_device_ids=true | all-gather | bytes 17408 | tf_op jit(solution)/shard_map/all_gather | solution.py:92
  107.4 0.4 fusion.19
  107.8 2.1 %collective-permute-start.1 = (bf16[64,2048]{1,0:T(8,128)(2,1)S(1)}, bf16[64,2048]{1,0:T(8,128)(2,1)S(1)}, u32[]{:S(2)}, u32[]{:S(2)}) collective-permute-start(bf16[64,2048]{1,0:T(8,128)(2,1)S(1)} %fusion.15), channel_id=1, source_target_pairs={{0,1},{1,0},{2,3},{3,2},{4,5},{5,4},{6,7},{7,6},{8,9},{9,8},{10,11... | collective-permute-start | bytes 786440 | tf_op jit(solution)/shard_map/ppermute | solution.py:31
  109.9 0.0 all-to-all-done.1
  109.9 0.3 fusion.10
  110.3 0.3 convolution_add_fusion
  110.7 2.2 %collective-permute-start.8 = (bf16[64,2048]{1,0:T(8,128)(2,1)S(1)}, bf16[64,2048]{1,0:T(8,128)(2,1)S(1)}, u32[]{:S(2)}, u32[]{:S(2)}) collective-permute-start(bf16[64,2048]{1,0:T(8,128)(2,1)S(1)} %fusion.16), channel_id=1, source_target_pairs={{0,1},{1,0},{2,3},{3,2},{4,5},{5,4},{6,7},{7,6},{8,9},{9,8},{10,11... | collective-permute-start | bytes 786440 | tf_op jit(solution)/shard_map/ppermute | solution.py:31
  112.9 0.1 fusion.17
  113.0 1.1 collective-permute-done.8
  114.1 0.1 fusion.18
  114.1 0.1 pad_maximum_fusion.1
  114.2 20.7 %all_to_all.20 = bf16[8,2,8,2048]{3,2,1,0:T(8,128)(2,1)S(1)} all-to-all(bf16[8,2,8,2048]{3,2,1,0:T(8,128)(2,1)S(1)} %pad_maximum_fusion.1), channel_id=1, replica_groups=mesh['ep'=32,'y2'=2,'y1'=2,'y0'=2,'c'=2] {'y2','y1','y0'}, dimensions={0} | all-to-all | bytes 1048576 | tf_op jit(solution)/shard_map/all_to_all | solution.py:35
  134.9 0.1 reduce_sum.62
  135.0 17.7 %all_to_all.21 = bf16[8,2,8,2048]{3,2,1,0:T(8,128)(2,1)S(1)} all-to-all(bf16[8,2,8,2048]{3,2,1,0:T(8,128)(2,1)S(1)} %broadcast_in_dim.2), channel_id=1, replica_groups=mesh['ep'=32,'y2'=2,'y1'=2,'y0'=2,'c'=2] {'y2','y1','y0'}, dimensions={0} | all-to-all | bytes 1048576 | tf_op jit(solution)/shard_map/all_to_all | solution.py:35
  152.8 5.0 %collective-permute-start.9 = (bf16[8,2,8,2048]{3,2,1,0:T(8,128)(2,1)S(1)}, bf16[8,2,8,2048]{3,2,1,0:T(8,128)(2,1)S(1)}, u32[]{:S(2)}, u32[]{:S(2)}) collective-permute-start(bf16[8,2,8,2048]{3,2,1,0:T(8,128)(2,1)S(1)} %all_to_all.21), channel_id=1, source_target_pairs={{0,1},{1,0},{2,3},{3,2},{4,5},{5,4},{6,7},{7,6},{8,9},{9,8},{10,11... | collective-permute-start | bytes 1572872 | tf_op jit(solution)/shard_map/ppermute | solution.py:31
  157.8 1.5 collective-permute-done.9
  159.3 0.1 select_bitcast_fusion.1
  159.4 1.0 pad_maximum_fusion.2
  (33 shorter events, 0.3 us)
Async XLA Ops:
  0.6 106.7 %copy-start = (bf16[96,2048]{1,0:T(8,128)(2,1)S(1)}, bf16[96,2048]{1,0:T(8,128)(2,1)}, u32[]{:S(2)}) copy-start(bf16[96,2048]{1,0:T(8,128)(2,1)} %param.20) | copy-start | bytes 1179652
  0.6 5.6 %copy-start.1 = (bf16[128,2048]{1,0:T(8,128)(2,1)S(1)}, bf16[128,2048]{1,0:T(8,128)(2,1)}, u32[]{:S(2)}) copy-start(bf16[128,2048]{1,0:T(8,128)(2,1)} %x_ref.1) | copy-start | bytes 1572868
  0.7 5.6 %copy-start.3 = (f32[2048]{0:T(1024)S(1)}, f32[2048]{0:T(1024)}, u32[]{:S(2)}) copy-start(f32[2048]{0:T(1024)} %param.22) | copy-start | bytes 24580
  0.7 5.6 %copy-start.4 = (s32[128,4]{0,1:T(4,128)S(1)}, s32[128,4]{0,1:T(4,128)}, u32[]{:S(2)}) copy-start(s32[128,4]{0,1:T(4,128)} %param.23) | copy-start | bytes 6148
  3.0 26.2 %collective-permute-start.3 = (bf16[2048,256]{1,0:T(8,128)(2,1)}, bf16[2048,256]{1,0:T(8,128)(2,1)}, u32[]{:S(2)}, u32[]{:S(2)}) collective-permute-start(bf16[2048,256]{1,0:T(8,128)(2,1)} %pad_maximum_fusion.refs_0_), channel_id=1, source_target_pairs={{0,2},{2,0},{1,3},{3,1},{4,6},{6,4},{5,7},{7,5},{8,10},{10,8},{9,1... | collective-permute-start | bytes 3145736 | tf_op jit(solution)/shard_map/ppermute | solution.py:31
  8.1 12.2 %copy-start.2 = (bf16[1,128,2048]{2,1,0:T(8,128)(2,1)S(1)}, bf16[1,128,2048]{2,1,0:T(8,128)(2,1)}, u32[]{:S(2)}) copy-start(bf16[1,128,2048]{2,1,0:T(8,128)(2,1)} %param.27) | copy-start | bytes 1572868
  8.1 27.7 %copy-start.6 = (bf16[128,2048]{1,0:T(8,128)(2,1)S(1)}, bf16[128,2048]{1,0:T(8,128)(2,1)}, u32[]{:S(2)}) copy-start(bf16[128,2048]{1,0:T(8,128)(2,1)} %param.14) | copy-start | bytes 1572868
  8.1 37.6 %all-to-all-start = ((bf16[32,8,2048]{2,1,0:T(8,128)(2,1)}), bf16[32,8,2048]{2,1,0:T(8,128)(2,1)}, u32[]{:S(2)}, u32[]{:S(2)}) async-start(bf16[32,8,2048]{2,1,0:T(8,128)(2,1)} %bitcast.44), calls=%async_computation | async-start | bytes 2097152 | tf_op jit(solution)/shard_map/all_to_all | solution.py:35
  20.3 20.2 %collective-permute-start.6 = (bf16[128,2048]{1,0:T(8,128)(2,1)S(1)}, bf16[128,2048]{1,0:T(8,128)(2,1)S(1)}, u32[]{:S(2)}, u32[]{:S(2)}) collective-permute-start(bf16[128,2048]{1,0:T(8,128)(2,1)S(1)} %bitcast.126), channel_id=1, source_target_pairs={{0,2},{2,0},{1,3},{3,1},{4,6},{6,4},{5,7},{7,5},{8,10},{10,8},{9,1... | collective-permute-start | bytes 1572872 | tf_op jit(solution)/shard_map/ppermute | solution.py:31
  22.4 23.0 %collective-permute-start.2 = (bf16[2048,256]{1,0:T(8,128)(2,1)}, bf16[2048,256]{1,0:T(8,128)(2,1)}, u32[]{:S(2)}, u32[]{:S(2)}) collective-permute-start(bf16[2048,256]{1,0:T(8,128)(2,1)} %pad_maximum_fusion.refs_0_), channel_id=1, source_target_pairs={{0,1},{1,0},{2,3},{3,2},{4,5},{5,4},{6,7},{7,6},{8,9},{9,8},{10,11... | collective-permute-start | bytes 3145736 | tf_op jit(solution)/shard_map/ppermute | solution.py:31
  29.3 16.4 %collective-permute-start.4 = (bf16[2048,256]{1,0:T(8,128)(2,1)}, bf16[2048,256]{1,0:T(8,128)(2,1)}, u32[]{:S(2)}, u32[]{:S(2)}) collective-permute-start(bf16[2048,256]{1,0:T(8,128)(2,1)} %collective-permute-done.3.refs_2_), channel_id=1, source_target_pairs={{0,1},{1,0},{2,3},{3,2},{4,5},{5,4},{6,7},{7,6},{8,9},{9,8},{10,11... | collective-permute-start | bytes 3145736 | tf_op jit(solution)/shard_map/ppermute | solution.py:31
  33.8 10.3 %collective-permute-start.5 = (bf16[128,2048]{1,0:T(8,128)(2,1)S(1)}, bf16[128,2048]{1,0:T(8,128)(2,1)S(1)}, u32[]{:S(2)}, u32[]{:S(2)}) collective-permute-start(bf16[128,2048]{1,0:T(8,128)(2,1)S(1)} %bitcast.127), channel_id=1, source_target_pairs={{0,1},{1,0},{2,3},{3,2},{4,5},{5,4},{6,7},{7,6},{8,9},{9,8},{10,11... | collective-permute-start | bytes 1572872 | tf_op jit(solution)/shard_map/ppermute | solution.py:31
  40.5 4.8 %collective-permute-start.7 = (bf16[128,2048]{1,0:T(8,128)(2,1)S(1)}, bf16[128,2048]{1,0:T(8,128)(2,1)S(1)}, u32[]{:S(2)}, u32[]{:S(2)}) collective-permute-start(bf16[128,2048]{1,0:T(8,128)(2,1)S(1)} %collective-permute-done.6.refs_6_), channel_id=1, source_target_pairs={{0,1},{1,0},{2,3},{3,2},{4,5},{5,4},{6,7},{7,6},{8,9},{9,8},{10,11... | collective-permute-start | bytes 1572872 | tf_op jit(solution)/shard_map/ppermute | solution.py:31
  51.0 11.9 %copy-start.9 = (bf16[2048,96]{0,1:T(8,128)(2,1)S(1)}, bf16[2048,96]{0,1:T(8,128)(2,1)}, u32[]{:S(2)}) copy-start(bf16[2048,96]{0,1:T(8,128)(2,1)} %param.16) | copy-start | bytes 1179652
  51.0 11.9 %copy-start.11 = (f32[2048]{0:T(1024)S(1)}, f32[2048]{0:T(1024)}, u32[]{:S(2)}) copy-start(f32[2048]{0:T(1024)} %param.15) | copy-start | bytes 24580
  51.0 58.9 %all-to-all-start.1 = ((bf16[32,8,2048]{2,1,0:T(8,128)(2,1)}), bf16[32,8,2048]{2,1,0:T(8,128)(2,1)S(1)}, u32[]{:S(2)}, u32[]{:S(2)}) async-start(bf16[32,8,2048]{2,1,0:T(8,128)(2,1)} %bitcast.133), calls=%async_computation.1 | async-start | bytes 2097152 | tf_op jit(solution)/shard_map/all_to_all | solution.py:35
  62.9 1.0 copy-start.10
  63.9 3.6 %copy-start.7 = (f32[31,96]{1,0:T(8,128)S(1)}, f32[31,96]{1,0:T(8,128)}, u32[]{:S(2)}) copy-start(f32[31,96]{1,0:T(8,128)} %param.18) | copy-start | bytes 35716
  63.9 3.6 %copy-start.5 = (f32[128,4]{0,1:T(4,128)S(1)}, f32[128,4]{0,1:T(4,128)}, u32[]{:S(2)}) copy-start(f32[128,4]{0,1:T(4,128)} %param.24) | copy-start | bytes 6148
  63.9 43.5 %copy-start.8 = (f32[96]{0:T(128)S(1)}, f32[96]{0:T(128)}, u32[]{:S(2)}) copy-start(f32[96]{0:T(128)} %param.19) | copy-start | bytes 1156
  64.4 22.6 %collective-permute-start = (bf16[30,96]{0,1:T(8,128)(2,1)S(1)}, bf16[30,96]{0,1:T(8,128)(2,1)S(1)}, u32[]{:S(2)}, u32[]{:S(2)}) collective-permute-start(bf16[30,96]{0,1:T(8,128)(2,1)S(1)} %slice.272), channel_id=1, source_target_pairs={{0,16},{16,32},{32,48},{48,64},{64,80},{80,96},{96,112},{112,128},... | collective-permute-start | bytes 17288 | tf_op jit(solution)/shard_map/ppermute | solution.py:27
  107.8 5.1 %collective-permute-start.1 = (bf16[64,2048]{1,0:T(8,128)(2,1)S(1)}, bf16[64,2048]{1,0:T(8,128)(2,1)S(1)}, u32[]{:S(2)}, u32[]{:S(2)}) collective-permute-start(bf16[64,2048]{1,0:T(8,128)(2,1)S(1)} %fusion.15), channel_id=1, source_target_pairs={{0,1},{1,0},{2,3},{3,2},{4,5},{5,4},{6,7},{7,6},{8,9},{9,8},{10,11... | collective-permute-start | bytes 786440 | tf_op jit(solution)/shard_map/ppermute | solution.py:31
  110.7 3.4 %collective-permute-start.8 = (bf16[64,2048]{1,0:T(8,128)(2,1)S(1)}, bf16[64,2048]{1,0:T(8,128)(2,1)S(1)}, u32[]{:S(2)}, u32[]{:S(2)}) collective-permute-start(bf16[64,2048]{1,0:T(8,128)(2,1)S(1)} %fusion.16), channel_id=1, source_target_pairs={{0,1},{1,0},{2,3},{3,2},{4,5},{5,4},{6,7},{7,6},{8,9},{9,8},{10,11... | collective-permute-start | bytes 786440 | tf_op jit(solution)/shard_map/ppermute | solution.py:31
  152.8 6.6 %collective-permute-start.9 = (bf16[8,2,8,2048]{3,2,1,0:T(8,128)(2,1)S(1)}, bf16[8,2,8,2048]{3,2,1,0:T(8,128)(2,1)S(1)}, u32[]{:S(2)}, u32[]{:S(2)}) collective-permute-start(bf16[8,2,8,2048]{3,2,1,0:T(8,128)(2,1)S(1)} %all_to_all.21), channel_id=1, source_target_pairs={{0,1},{1,0},{2,3},{3,2},{4,5},{5,4},{6,7},{7,6},{8,9},{9,8},{10,11... | collective-permute-start | bytes 1572872 | tf_op jit(solution)/shard_map/ppermute | solution.py:31

commit v2 on v1

--- a/solution.py
+++ b/solution.py
@@ -124,8 +124,11 @@
     return jnp.dot(spread, place, preferred_element_type=jnp.float32) == slot.astype(jnp.float32)
 
 
-def front_kernel(member, x_ref, gain_ref, ids_ref, rows_ref):
+def front_kernel(member, x_ref, gain_ref, ids_ref, gate_ref, up_ref, rows_ref, both_ref):
     rows = x_ref.shape[0]
+    inner = gate_ref.shape[1]
+    both_ref[:, :inner] = gate_ref[...]
+    both_ref[:, inner:] = up_ref[...]
     sent = rows_ref.shape[0]
     slots = sent // EXPERTS
     normed = row_norm(x_ref[...], gain_ref[...]).astype(jnp.bfloat16)
@@ -135,17 +138,21 @@
     rows_ref[...] = jnp.dot(select, normed, preferred_element_type=jnp.float32).astype(jnp.bfloat16)
 
 
-def front(member, x, gain, ids, sent):
+def front(member, x, gain, ids, gate, up, sent):
     _, width = x.shape
+    inner = gate.shape[1]
     whole = pl.BlockSpec(memory_space=pltpu.VMEM)
     return pl.pallas_call(
         front_kernel,
-        in_specs=[pl.BlockSpec(memory_space=pltpu.SMEM)] + [whole] * 3,
-        out_specs=whole,
-        out_shape=jax.ShapeDtypeStruct((sent, width), jnp.bfloat16),
-        compiler_params=pltpu.CompilerParams(vmem_limit_bytes=8 << 20),
+        in_specs=[pl.BlockSpec(memory_space=pltpu.SMEM)] + [whole] * 5,
+        out_specs=[whole] * 2,
+        out_shape=[
+            jax.ShapeDtypeStruct((sent, width), jnp.bfloat16),
+            jax.ShapeDtypeStruct((width, 2 * inner), jnp.bfloat16),
+        ],
+        compiler_params=pltpu.CompilerParams(vmem_limit_bytes=57000 << 10),
         name="front",
-    )(member.reshape(1), x, gain.reshape(1, width), ids)
+    )(member.reshape(1), x, gain.reshape(1, width), ids, gate, up)
 
 
 def mixing_kernel(member, ids_ref, scores_ref, hi_ref, lo_ref):
@@ -233,7 +240,10 @@
     slots = capacity // GROUP
     member = lax.axis_index(("y0", "c")).astype(jnp.int32)
 
-    gate_up = jnp.concatenate([expert_gate[0], expert_up[0]], axis=1)
+    ids = route_experts.T
+    sending, gate_up = front(
+        member, expert_in, expert_gain, ids, expert_gate[0], expert_up[0], experts * slots
+    )
     down = expert_down[0]
     gu_y = swapped(gate_up, "y0")
     down_y = swapped(down, "y0")
@@ -242,8 +252,6 @@
     gu_d = swapped(gu_y, "c")
     down_d = swapped(down_y, "c")
 
-    ids = route_experts.T
-    sending = front(member, expert_in, expert_gain, ids, experts * slots)
     arrived = exchanged(sending.reshape(experts, slots, width), "ep").reshape(-1, width)
 
     mixing_hi, mixing_lo = mixing(member, ids, route_scores.T, experts * slots)

time: 161 us -> 164 us (1.019)
  local copies, waits for them, and re-layouts: 0.85 us -> 4.14 us
  other arithmetic: 5.06 us -> 2.7 us
  Pallas kernels: 7.41 us -> 9.19 us
    unnamed x24 -> x28, local copies, waits for them, and re-layouts: 0.63 us -> 3.92 us
    concatenate x1 -> x0, other arithmetic: 2.36 us -> none  [program(): gate_up = jnp.concatenate([expert_gate[0], expert_up[0]], axis=1)]
    pallas_call x1, Pallas kernels: 1.79 us -> 3.57 us  [front(): pl.pallas_call(front_kernel, in_specs=[pl.BlockSpec(memory_space=pltpu.SM...]
  transfers between devices with their start and end apart: 12 -> 12, of which waited for: 7 -> 6; matrix products, arithmetic and copies ran while one was open for 2% -> 2% of each run, Pallas kernels for 1% -> 0%
where the time goes in v2:
time: 164 us; the launch traced here: 163 us
  blocking collectives  57.9 us (35%)
  starting transfers between devices  55.8 us (34%)
  waiting for transfers between devices  30.6 us (19%)
  Pallas kernels  9.19 us (6%)
  local copies, waits for them, and re-layouts  4.14 us (3%)
  other arithmetic  2.7 us (2%)
  matrix products  1.9 us (1%)
    all_to_all x2, blocking collectives, exchanged(): return lax.all_to_all(x, axis, split_axis=0, concat_axis=0, tiled=True)  38.4 us
    ppermute x9, starting transfers between devices, swapped(): return lax.ppermute(x, axis, [(0, 1), (1, 0)])  28.4 us
    all_to_all x2, starting transfers between devices, exchanged(): return lax.all_to_all(x, axis, split_axis=0, concat_axis=0, tiled=True)  24.3 us
    all_gather x1, blocking collectives, projected(): everyone = lax.all_gather(sums, TP)  19.5 us
    ppermute x1, waiting for transfers between devices, shifted(): return lax.ppermute(block, axis, route)  18.4 us
    ppermute x9, waiting for transfers between devices, swapped(): return lax.ppermute(x, axis, [(0, 1), (1, 0)])  12.2 us
    pallas_call x1, Pallas kernels, expert(): pl.pallas_call(expert_kernel, in_specs=[whole] * (1 + 2 * GROUP), out_spe...  5.3 us
    unnamed x28, local copies, waits for them, and re-layouts  3.92 us
  transfers between devices with their start and end apart: 12, of which 6 were waited for; matrix products, arithmetic and copies ran while one was open for 2% of the time, Pallas kernels for 0%

profile of v2, /device:TPU:65, one launch (start us, length us, event | category | flops | bytes accessed | tf_op | source)
XLA Modules:
  0.0 163.2 jit_solution(5714228957053521439)
XLA Ops:
  0.6 0.0 copy-start
  0.7 3.6 %front.1 = (bf16[256,2048]{1,0:T(8,128)(2,1)}, bf16[2048,256]{1,0:T(8,128)(2,1)}) custom-call(s32[1]{0:T(128)} %bitcast.40.member, bf16[128,2048]{1,0:T(8,128)(2,1)} %x_ref.1, f32[1,2048]{1,0:T(1,128)} %bitcast.141, s32[4,128]{1,0:T(4,128)} %bitcast.129, bf16[2048,128]{1,0:T(8,128)(2,1)} %bitcast.139, bf16[2048,128]{1,0:T(8,128)(2,1)} %bitcast.140), custom_call_target="tpu_custom_call" | custom-call | tf_op jit(solution)/shard_map/front/pallas_call | solution.py:145
  4.2 3.2 %collective-permute-start.3 = (bf16[2048,256]{1,0:T(8,128)(2,1)}, bf16[2048,256]{1,0:T(8,128)(2,1)}, u32[]{:S(2)}, u32[]{:S(2)}) collective-permute-start(bf16[2048,256]{1,0:T(8,128)(2,1)} %get-tuple-element.8.refs_0_), channel_id=1, source_target_pairs={{0,2},{2,0},{1,3},{3,1},{4,6},{6,4},{5,7},{7,5},{8,10},{10,8},{9,1... | collective-permute-start | bytes 3145736 | tf_op jit(solution)/shard_map/ppermute | solution.py:31
  7.4 0.0 copy-start.1
  7.4 0.0 copy-start.5
  7.5 12.2 %all-to-all-start = ((bf16[32,8,2048]{2,1,0:T(8,128)(2,1)}), bf16[32,8,2048]{2,1,0:T(8,128)(2,1)S(1)}, u32[]{:S(2)}, u32[]{:S(2)}) async-start(bf16[32,8,2048]{2,1,0:T(8,128)(2,1)} %bitcast.138), calls=%async_computation | async-start | bytes 2097152 | tf_op jit(solution)/shard_map/all_to_all | solution.py:35
  19.6 2.2 %collective-permute-start.6 = (bf16[128,2048]{1,0:T(8,128)(2,1)S(1)}, bf16[128,2048]{1,0:T(8,128)(2,1)S(1)}, u32[]{:S(2)}, u32[]{:S(2)}) collective-permute-start(bf16[128,2048]{1,0:T(8,128)(2,1)S(1)} %bitcast.126), channel_id=1, source_target_pairs={{0,2},{2,0},{1,3},{3,1},{4,6},{6,4},{5,7},{7,5},{8,10},{10,8},{9,1... | collective-permute-start | bytes 1572872 | tf_op jit(solution)/shard_map/ppermute | solution.py:31
  21.9 3.7 %collective-permute-start.2 = (bf16[2048,256]{1,0:T(8,128)(2,1)}, bf16[2048,256]{1,0:T(8,128)(2,1)S(1)}, u32[]{:S(2)}, u32[]{:S(2)}) collective-permute-start(bf16[2048,256]{1,0:T(8,128)(2,1)} %get-tuple-element.8.refs_0_), channel_id=1, source_target_pairs={{0,1},{1,0},{2,3},{3,2},{4,5},{5,4},{6,7},{7,6},{8,9},{9,8},{10,11... | collective-permute-start | bytes 3145736 | tf_op jit(solution)/shard_map/ppermute | solution.py:31
  25.6 4.9 %collective-permute-done.3.refs_2_ = bf16[2048,256]{1,0:T(8,128)(2,1)} collective-permute-done((bf16[2048,256]{1,0:T(8,128)(2,1)}, bf16[2048,256]{1,0:T(8,128)(2,1)}, u32[]{:S(2)}, u32[]{:S(2)}) %collective-permute-start.3) | collective-permute-done | bytes 1048608 | tf_op jit(solution)/shard_map/ppermute | solution.py:31
  30.5 4.6 %collective-permute-start.4 = (bf16[2048,256]{1,0:T(8,128)(2,1)}, bf16[2048,256]{1,0:T(8,128)(2,1)}, u32[]{:S(2)}, u32[]{:S(2)}) collective-permute-start(bf16[2048,256]{1,0:T(8,128)(2,1)} %collective-permute-done.3.refs_2_), channel_id=1, source_target_pairs={{0,1},{1,0},{2,3},{3,2},{4,5},{5,4},{6,7},{7,6},{8,9},{9,8},{10,11... | collective-permute-start | bytes 3145736 | tf_op jit(solution)/shard_map/ppermute | solution.py:31
  35.0 1.9 %collective-permute-start.5 = (bf16[128,2048]{1,0:T(8,128)(2,1)S(1)}, bf16[128,2048]{1,0:T(8,128)(2,1)S(1)}, u32[]{:S(2)}, u32[]{:S(2)}) collective-permute-start(bf16[128,2048]{1,0:T(8,128)(2,1)S(1)} %bitcast.127), channel_id=1, source_target_pairs={{0,1},{1,0},{2,3},{3,2},{4,5},{5,4},{6,7},{7,6},{8,9},{9,8},{10,11... | collective-permute-start | bytes 1572872 | tf_op jit(solution)/shard_map/ppermute | solution.py:31
  37.0 0.2 convert_reduce_fusion
  37.1 4.5 %collective-permute-done.6.refs_6_ = bf16[128,2048]{1,0:T(8,128)(2,1)S(1)} collective-permute-done((bf16[128,2048]{1,0:T(8,128)(2,1)S(1)}, bf16[128,2048]{1,0:T(8,128)(2,1)S(1)}, u32[]{:S(2)}, u32[]{:S(2)}) %collective-permute-start.6) | collective-permute-done | bytes 524320 | tf_op jit(solution)/shard_map/ppermute | solution.py:31
  41.6 3.4 %collective-permute-start.7 = (bf16[128,2048]{1,0:T(8,128)(2,1)S(1)}, bf16[128,2048]{1,0:T(8,128)(2,1)S(1)}, u32[]{:S(2)}, u32[]{:S(2)}) collective-permute-start(bf16[128,2048]{1,0:T(8,128)(2,1)S(1)} %collective-permute-done.6.refs_6_), channel_id=1, source_target_pairs={{0,1},{1,0},{2,3},{3,2},{4,5},{5,4},{6,7},{7,6},{8,9},{9,8},{10,11... | collective-permute-start | bytes 1572872 | tf_op jit(solution)/shard_map/ppermute | solution.py:31
  45.1 0.3 fusion.7
  45.4 1.0 copy-done.8
  46.4 0.2 collective-permute-done.7.refs_7_
  46.6 1.0 copy-done.4
  47.5 5.3 %expert.1 = bf16[256,2048]{1,0:T(8,128)(2,1)} custom-call(bf16[256,2048]{1,0:T(8,128)(2,1)} %bitcast.133, bf16[2048,256]{1,0:T(8,128)(2,1)} %get-tuple-element.8.refs_0_, bf16[2048,256]{1,0:T(8,128)(2,1)} %copy-done.8, bf16[2048,256]{1,0:T(8,128)(2,1)} %collective-permute-done.3.refs_2_, bf16[2048,256]{1,0:T(8,128)(2,1)} %collective-permute-done.4.refs_3_, ...), custom_call_target="tpu_custom_call" | custom-call | tf_op jit(solution)/shard_map/expert/pallas_call | solution.py:211
  52.8 12.2 %all-to-all-start.1 = ((bf16[32,8,2048]{2,1,0:T(8,128)(2,1)}), bf16[32,8,2048]{2,1,0:T(8,128)(2,1)S(1)}, u32[]{:S(2)}, u32[]{:S(2)}) async-start(bf16[32,8,2048]{2,1,0:T(8,128)(2,1)} %bitcast.132), calls=%async_computation.1 | async-start | bytes 2097152 | tf_op jit(solution)/shard_map/all_to_all | solution.py:35
  65.1 0.4 fusion.57
  65.5 0.6 copy-done.12
  66.0 0.4 fusion.6
  66.5 0.1 slice.272
  66.6 3.1 %collective-permute-start = (bf16[30,96]{0,1:T(8,128)(2,1)S(1)}, bf16[30,96]{0,1:T(8,128)(2,1)S(1)}, u32[]{:S(2)}, u32[]{:S(2)}) collective-permute-start(bf16[30,96]{0,1:T(8,128)(2,1)S(1)} %slice.272), channel_id=1, source_target_pairs={{0,16},{16,32},{32,48},{48,64},{64,80},{80,96},{96,112},{112,128},... | collective-permute-start | bytes 17288 | tf_op jit(solution)/shard_map/ppermute | solution.py:27
  69.7 0.6 copy-done.3
  70.4 0.0 copy-done.2
  70.4 0.3 mixing.1
  70.7 18.4 %collective-permute-done = bf16[30,96]{0,1:T(8,128)(2,1)S(1)} collective-permute-done((bf16[30,96]{0,1:T(8,128)(2,1)S(1)}, bf16[30,96]{0,1:T(8,128)(2,1)S(1)}, u32[]{:S(2)}, u32[]{:S(2)}) %collective-permute-start) | collective-permute-done | bytes 5792 | tf_op jit(solution)/shard_map/ppermute | solution.py:27
  89.1 0.9 fusion.59
  90.0 19.5 %all-gather.1 = f32[16,2,128]{2,1,0:T(2,128)S(1)} all-gather(f32[1,2,128]{2,1,0:T(2,128)S(1)} %maximum_bitcast_fusion), channel_id=2, replica_groups=mesh['ep'=32,'y2'=2,'y1'=2,'y0'=2,'c'=2] {'y2','y1','y0','c'}, dimensions={0}, use_global_device_ids=true | all-gather | bytes 17408 | tf_op jit(solution)/shard_map/all_gather | solution.py:92
  109.6 0.6 copy-done.10
  110.2 0.4 fusion.19
  110.7 2.1 %collective-permute-start.1 = (bf16[64,2048]{1,0:T(8,128)(2,1)S(1)}, bf16[64,2048]{1,0:T(8,128)(2,1)S(1)}, u32[]{:S(2)}, u32[]{:S(2)}) collective-permute-start(bf16[64,2048]{1,0:T(8,128)(2,1)S(1)} %fusion.15), channel_id=1, source_target_pairs={{0,1},{1,0},{2,3},{3,2},{4,5},{5,4},{6,7},{7,6},{8,9},{9,8},{10,11... | collective-permute-start | bytes 786440 | tf_op jit(solution)/shard_map/ppermute | solution.py:31
  112.7 0.3 fusion.10
  113.1 0.3 convolution_add_fusion
  113.5 2.3 %collective-permute-start.8 = (bf16[64,2048]{1,0:T(8,128)(2,1)S(1)}, bf16[64,2048]{1,0:T(8,128)(2,1)S(1)}, u32[]{:S(2)}, u32[]{:S(2)}) collective-permute-start(bf16[64,2048]{1,0:T(8,128)(2,1)S(1)} %fusion.16), channel_id=1, source_target_pairs={{0,1},{1,0},{2,3},{3,2},{4,5},{5,4},{6,7},{7,6},{8,9},{9,8},{10,11... | collective-permute-start | bytes 786440 | tf_op jit(solution)/shard_map/ppermute | solution.py:31
  115.7 0.1 fusion.17
  115.8 1.1 collective-permute-done.8
  116.9 0.1 fusion.18
  117.0 0.1 pad_maximum_fusion
  117.0 20.7 %all_to_all.20 = bf16[8,2,8,2048]{3,2,1,0:T(8,128)(2,1)S(1)} all-to-all(bf16[8,2,8,2048]{3,2,1,0:T(8,128)(2,1)S(1)} %pad_maximum_fusion), channel_id=1, replica_groups=mesh['ep'=32,'y2'=2,'y1'=2,'y0'=2,'c'=2] {'y2','y1','y0'}, dimensions={0} | all-to-all | bytes 1048576 | tf_op jit(solution)/shard_map/all_to_all | solution.py:35
  137.7 0.1 reduce_sum.62
  137.8 17.7 %all_to_all.21 = bf16[8,2,8,2048]{3,2,1,0:T(8,128)(2,1)S(1)} all-to-all(bf16[8,2,8,2048]{3,2,1,0:T(8,128)(2,1)S(1)} %broadcast_in_dim.2), channel_id=1, replica_groups=mesh['ep'=32,'y2'=2,'y1'=2,'y0'=2,'c'=2] {'y2','y1','y0'}, dimensions={0} | all-to-all | bytes 1048576 | tf_op jit(solution)/shard_map/all_to_all | solution.py:35
  155.5 5.1 %collective-permute-start.9 = (bf16[8,2,8,2048]{3,2,1,0:T(8,128)(2,1)S(1)}, bf16[8,2,8,2048]{3,2,1,0:T(8,128)(2,1)S(1)}, u32[]{:S(2)}, u32[]{:S(2)}) collective-permute-start(bf16[8,2,8,2048]{3,2,1,0:T(8,128)(2,1)S(1)} %all_to_all.21), channel_id=1, source_target_pairs={{0,1},{1,0},{2,3},{3,2},{4,5},{5,4},{6,7},{7,6},{8,9},{9,8},{10,11... | collective-permute-start | bytes 1572872 | tf_op jit(solution)/shard_map/ppermute | solution.py:31
  160.6 1.5 collective-permute-done.9
  162.1 0.1 select_bitcast_fusion.1
  162.2 1.0 pad_maximum_fusion.1
  (36 shorter events, 0.3 us)
Async XLA Ops:
  0.6 108.9 %copy-start = (bf16[96,2048]{1,0:T(8,128)(2,1)S(1)}, bf16[96,2048]{1,0:T(8,128)(2,1)}, u32[]{:S(2)}) copy-start(bf16[96,2048]{1,0:T(8,128)(2,1)} %param.20) | copy-start | bytes 1179652
  4.2 26.2 %collective-permute-start.3 = (bf16[2048,256]{1,0:T(8,128)(2,1)}, bf16[2048,256]{1,0:T(8,128)(2,1)}, u32[]{:S(2)}, u32[]{:S(2)}) collective-permute-start(bf16[2048,256]{1,0:T(8,128)(2,1)} %get-tuple-element.8.refs_0_), channel_id=1, source_target_pairs={{0,2},{2,0},{1,3},{3,1},{4,6},{6,4},{5,7},{7,5},{8,10},{10,8},{9,1... | collective-permute-start | bytes 3145736 | tf_op jit(solution)/shard_map/ppermute | solution.py:31
  7.4 12.2 %copy-start.1 = (bf16[1,128,2048]{2,1,0:T(8,128)(2,1)S(1)}, bf16[1,128,2048]{2,1,0:T(8,128)(2,1)}, u32[]{:S(2)}) copy-start(bf16[1,128,2048]{2,1,0:T(8,128)(2,1)} %param.27) | copy-start | bytes 1572868
  7.4 29.5 %copy-start.5 = (bf16[128,2048]{1,0:T(8,128)(2,1)S(1)}, bf16[128,2048]{1,0:T(8,128)(2,1)}, u32[]{:S(2)}) copy-start(bf16[128,2048]{1,0:T(8,128)(2,1)} %param.14) | copy-start | bytes 1572868
  7.5 39.1 %all-to-all-start = ((bf16[32,8,2048]{2,1,0:T(8,128)(2,1)}), bf16[32,8,2048]{2,1,0:T(8,128)(2,1)S(1)}, u32[]{:S(2)}, u32[]{:S(2)}) async-start(bf16[32,8,2048]{2,1,0:T(8,128)(2,1)} %bitcast.138), calls=%async_computation | async-start | bytes 2097152 | tf_op jit(solution)/shard_map/all_to_all | solution.py:35
  19.6 25.4 %copy-start.6 = (bf16[128,2048]{1,0:T(8,128)(2,1)S(1)}, bf16[128,2048]{1,0:T(8,128)(2,1)}, u32[]{:S(2)}) copy-start(bf16[128,2048]{1,0:T(8,128)(2,1)} %param.14) | copy-start | bytes 1572868
  19.6 22.0 %collective-permute-start.6 = (bf16[128,2048]{1,0:T(8,128)(2,1)S(1)}, bf16[128,2048]{1,0:T(8,128)(2,1)S(1)}, u32[]{:S(2)}, u32[]{:S(2)}) collective-permute-start(bf16[128,2048]{1,0:T(8,128)(2,1)S(1)} %bitcast.126), channel_id=1, source_target_pairs={{0,2},{2,0},{1,3},{3,1},{4,6},{6,4},{5,7},{7,5},{8,10},{10,8},{9,1... | collective-permute-start | bytes 1572872 | tf_op jit(solution)/shard_map/ppermute | solution.py:31
  21.9 23.5 %collective-permute-start.2 = (bf16[2048,256]{1,0:T(8,128)(2,1)}, bf16[2048,256]{1,0:T(8,128)(2,1)S(1)}, u32[]{:S(2)}, u32[]{:S(2)}) collective-permute-start(bf16[2048,256]{1,0:T(8,128)(2,1)} %get-tuple-element.8.refs_0_), channel_id=1, source_target_pairs={{0,1},{1,0},{2,3},{3,2},{4,5},{5,4},{6,7},{7,6},{8,9},{9,8},{10,11... | collective-permute-start | bytes 3145736 | tf_op jit(solution)/shard_map/ppermute | solution.py:31
  30.5 16.1 %collective-permute-start.4 = (bf16[2048,256]{1,0:T(8,128)(2,1)}, bf16[2048,256]{1,0:T(8,128)(2,1)}, u32[]{:S(2)}, u32[]{:S(2)}) collective-permute-start(bf16[2048,256]{1,0:T(8,128)(2,1)} %collective-permute-done.3.refs_2_), channel_id=1, source_target_pairs={{0,1},{1,0},{2,3},{3,2},{4,5},{5,4},{6,7},{7,6},{8,9},{9,8},{10,11... | collective-permute-start | bytes 3145736 | tf_op jit(solution)/shard_map/ppermute | solution.py:31
  35.0 10.3 %collective-permute-start.5 = (bf16[128,2048]{1,0:T(8,128)(2,1)S(1)}, bf16[128,2048]{1,0:T(8,128)(2,1)S(1)}, u32[]{:S(2)}, u32[]{:S(2)}) collective-permute-start(bf16[128,2048]{1,0:T(8,128)(2,1)S(1)} %bitcast.127), channel_id=1, source_target_pairs={{0,1},{1,0},{2,3},{3,2},{4,5},{5,4},{6,7},{7,6},{8,9},{9,8},{10,11... | collective-permute-start | bytes 1572872 | tf_op jit(solution)/shard_map/ppermute | solution.py:31
  41.6 4.9 %collective-permute-start.7 = (bf16[128,2048]{1,0:T(8,128)(2,1)S(1)}, bf16[128,2048]{1,0:T(8,128)(2,1)S(1)}, u32[]{:S(2)}, u32[]{:S(2)}) collective-permute-start(bf16[128,2048]{1,0:T(8,128)(2,1)S(1)} %collective-permute-done.6.refs_6_), channel_id=1, source_target_pairs={{0,1},{1,0},{2,3},{3,2},{4,5},{5,4},{6,7},{7,6},{8,9},{9,8},{10,11... | collective-permute-start | bytes 1572872 | tf_op jit(solution)/shard_map/ppermute | solution.py:31
  45.4 1.0 copy-start.8
  46.5 1.0 copy-start.4
  52.8 12.2 %copy-start.7 = (bf16[128,2048]{1,0:T(8,128)(2,1)S(1)}, bf16[128,2048]{1,0:T(8,128)(2,1)}, u32[]{:S(2)}) copy-start(bf16[128,2048]{1,0:T(8,128)(2,1)} %param.14) | copy-start | bytes 1572868
  52.8 12.2 %copy-start.11 = (bf16[2048,96]{0,1:T(8,128)(2,1)S(1)}, bf16[2048,96]{0,1:T(8,128)(2,1)}, u32[]{:S(2)}) copy-start(bf16[2048,96]{0,1:T(8,128)(2,1)} %param.16) | copy-start | bytes 1179652
  52.8 12.2 %copy-start.13 = (f32[2048]{0:T(1024)S(1)}, f32[2048]{0:T(1024)}, u32[]{:S(2)}) copy-start(f32[2048]{0:T(1024)} %param.15) | copy-start | bytes 24580
  52.8 59.9 %all-to-all-start.1 = ((bf16[32,8,2048]{2,1,0:T(8,128)(2,1)}), bf16[32,8,2048]{2,1,0:T(8,128)(2,1)S(1)}, u32[]{:S(2)}, u32[]{:S(2)}) async-start(bf16[32,8,2048]{2,1,0:T(8,128)(2,1)} %bitcast.132), calls=%async_computation.1 | async-start | bytes 2097152 | tf_op jit(solution)/shard_map/all_to_all | solution.py:35
  65.0 1.0 copy-start.12
  66.5 3.2 %copy-start.9 = (f32[31,96]{1,0:T(8,128)S(1)}, f32[31,96]{1,0:T(8,128)}, u32[]{:S(2)}) copy-start(f32[31,96]{1,0:T(8,128)} %param.18) | copy-start | bytes 35716
  66.6 22.6 %collective-permute-start = (bf16[30,96]{0,1:T(8,128)(2,1)S(1)}, bf16[30,96]{0,1:T(8,128)(2,1)S(1)}, u32[]{:S(2)}, u32[]{:S(2)}) collective-permute-start(bf16[30,96]{0,1:T(8,128)(2,1)S(1)} %slice.272), channel_id=1, source_target_pairs={{0,16},{16,32},{32,48},{48,64},{64,80},{80,96},{96,112},{112,128},... | collective-permute-start | bytes 17288 | tf_op jit(solution)/shard_map/ppermute | solution.py:27
  69.7 0.7 copy-start.3
  69.7 0.7 copy-start.2
  109.5 0.7 copy-start.10
  110.7 5.1 %collective-permute-start.1 = (bf16[64,2048]{1,0:T(8,128)(2,1)S(1)}, bf16[64,2048]{1,0:T(8,128)(2,1)S(1)}, u32[]{:S(2)}, u32[]{:S(2)}) collective-permute-start(bf16[64,2048]{1,0:T(8,128)(2,1)S(1)} %fusion.15), channel_id=1, source_target_pairs={{0,1},{1,0},{2,3},{3,2},{4,5},{5,4},{6,7},{7,6},{8,9},{9,8},{10,11... | collective-permute-start | bytes 786440 | tf_op jit(solution)/shard_map/ppermute | solution.py:31
  113.5 3.4 %collective-permute-start.8 = (bf16[64,2048]{1,0:T(8,128)(2,1)S(1)}, bf16[64,2048]{1,0:T(8,128)(2,1)S(1)}, u32[]{:S(2)}, u32[]{:S(2)}) collective-permute-start(bf16[64,2048]{1,0:T(8,128)(2,1)S(1)} %fusion.16), channel_id=1, source_target_pairs={{0,1},{1,0},{2,3},{3,2},{4,5},{5,4},{6,7},{7,6},{8,9},{9,8},{10,11... | collective-permute-start | bytes 786440 | tf_op jit(solution)/shard_map/ppermute | solution.py:31
  155.5 6.6 %collective-permute-start.9 = (bf16[8,2,8,2048]{3,2,1,0:T(8,128)(2,1)S(1)}, bf16[8,2,8,2048]{3,2,1,0:T(8,128)(2,1)S(1)}, u32[]{:S(2)}, u32[]{:S(2)}) collective-permute-start(bf16[8,2,8,2048]{3,2,1,0:T(8,128)(2,1)S(1)} %all_to_all.21), channel_id=1, source_target_pairs={{0,1},{1,0},{2,3},{3,2},{4,5},{5,4},{6,7},{7,6},{8,9},{9,8},{10,11... | collective-permute-start | bytes 1572872 | tf_op jit(solution)/shard_map/ppermute | solution.py:31

commit v3 on v1

--- a/solution.py
+++ b/solution.py
@@ -180,35 +180,36 @@
     )(member.reshape(1), ids, scores)
 
 
-def expert_kernel(x_ref, *refs):
-    gus, downs, out_ref = refs[:GROUP], refs[GROUP : 2 * GROUP], refs[2 * GROUP]
-    inner = downs[0].shape[0]
-    width = out_ref.shape[1]
-    hidden = []
-    for gu in gus:
+def hidden_kernel(x_ref, *refs):
+    gus, out_ref = refs[:GROUP], refs[GROUP]
+    inner = gus[0].shape[1] // 2
+    for at, gu in enumerate(gus):
         both = jnp.dot(x_ref[...], gu[...], preferred_element_type=jnp.float32)
         g = jnp.minimum(both[:, :inner], clamp_limit)
         u = jnp.clip(both[:, inner:], -clamp_limit, clamp_limit)
-        hidden.append(((u + 1.0) * g * jax.nn.sigmoid(swish_slope * g)).astype(jnp.bfloat16))
-    hidden = jnp.concatenate(hidden, axis=1)
+        hidden = (u + 1.0) * g * jax.nn.sigmoid(swish_slope * g)
+        out_ref[:, at * inner : (at + 1) * inner] = hidden.astype(jnp.bfloat16)
+
+
+def down_kernel(hidden_ref, *refs):
+    downs, out_ref = refs[:GROUP], refs[GROUP]
     step = 512
-    for at in range(0, width, step):
+    for at in range(0, out_ref.shape[1], step):
         weights = jnp.concatenate([down[:, at : at + step] for down in downs], axis=0)
         out_ref[:, at : at + step] = jnp.dot(
-            hidden, weights, preferred_element_type=jnp.float32
+            hidden_ref[...], weights, preferred_element_type=jnp.float32
         ).astype(jnp.bfloat16)
 
 
-def expert(x, gus, downs):
+def in_vmem(kernel, limit, shape, *operands):
     whole = pl.BlockSpec(memory_space=pltpu.VMEM)
     return pl.pallas_call(
-        expert_kernel,
-        in_specs=[whole] * (1 + 2 * GROUP),
+        kernel,
+        in_specs=[whole] * len(operands),
         out_specs=whole,
-        out_shape=jax.ShapeDtypeStruct(x.shape, jnp.bfloat16),
-        compiler_params=pltpu.CompilerParams(vmem_limit_bytes=53000 << 10),
-        name="expert",
-    )(x, *gus, *downs)
+        out_shape=jax.ShapeDtypeStruct(shape, jnp.bfloat16),
+        compiler_params=pltpu.CompilerParams(vmem_limit_bytes=limit << 10),
+    )(*operands)
 
 
 def program(
@@ -251,7 +252,9 @@
     mixer_partial = projected(conv_out, channel_gain, w_output)
     mixer_half = core_half(mixer_partial)
 
-    partial = expert(arrived, (gate_up, gu_c, gu_y, gu_d), (down, down_c, down_y, down_d))
+    hidden_shape = (experts * slots, GROUP * down.shape[0])
+    hidden = in_vmem(hidden_kernel, 53000, hidden_shape, arrived, gate_up, gu_c, gu_y, gu_d)
+    partial = in_vmem(down_kernel, 53000, arrived.shape, hidden, down, down_c, down_y, down_d)
     returned = exchanged(partial.reshape(experts, slots, width), "ep").reshape(-1, width)
 
     def mixed(m):

time: 161 us -> 162 us (level)
  other arithmetic: 5.06 us -> 7.15 us
    ppermute x9, waiting for transfers between devices: 11.6 us -> 9.33 us  [swapped(): return lax.ppermute(x, axis, [(0, 1), (1, 0)])]
    pallas_call x1 -> x2, Pallas kernels: 5.29 us -> 6.21 us  [in_vmem(): pl.pallas_call(kernel, in_specs=[whole] * len(operands), out_specs=whole,...]
  transfers between devices with their start and end apart: 12 -> 12, of which waited for: 7 -> 6; matrix products, arithmetic and copies ran while one was open for 2% -> 3% of each run, Pallas kernels for 1% -> 3%
where the time goes in v3:
time: 162 us
  blocking collectives  57.6 us (36%)
  starting transfers between devices  55.3 us (34%)
  waiting for transfers between devices  29.4 us (18%)
  Pallas kernels  8.29 us (5%)
  other arithmetic  7.15 us (4%)
  matrix products  1.9 us (1%)
    all_to_all x2, blocking collectives, exchanged(): return lax.all_to_all(x, axis, split_axis=0, concat_axis=0, tiled=True)  38.4 us
    ppermute x9, starting transfers between devices, swapped(): return lax.ppermute(x, axis, [(0, 1), (1, 0)])  28.2 us
    all_to_all x2, starting transfers between devices, exchanged(): return lax.all_to_all(x, axis, split_axis=0, concat_axis=0, tiled=True)  24 us
    ppermute x1, waiting for transfers between devices, shifted(): return lax.ppermute(block, axis, route)  19.7 us
    all_gather x1, blocking collectives, projected(): everyone = lax.all_gather(sums, TP)  19.1 us
    ppermute x9, waiting for transfers between devices, swapped(): return lax.ppermute(x, axis, [(0, 1), (1, 0)])  9.33 us
    pallas_call x2, Pallas kernels, in_vmem(): pl.pallas_call(kernel, in_specs=[whole] * len(operands), out_specs=whole,...  6.21 us
  transfers between devices with their start and end apart: 12, of which 6 were waited for; matrix products, arithmetic and copies ran while one was open for 3% of the time, Pallas kernels for 3%

profile of v3, /device:TPU:65, one launch (start us, length us, event | category | flops | bytes accessed | tf_op | source)
XLA Modules:
  0.0 161.5 jit_solution(16413700700725020905)
XLA Ops:
  0.6 0.0 copy-start
  0.7 2.4 %pad_maximum_fusion.refs_0_ = bf16[2048,256]{1,0:T(8,128)(2,1)} fusion(bf16[2048,128]{1,0:T(8,128)(2,1)} %bitcast.139, bf16[2048,128]{1,0:T(8,128)(2,1)} %bitcast.140), kind=kLoop, calls=%fused_computation.14 | loop fusion | flops 2097152 | bytes 2097152 | tf_op jit(solution)/shard_map/concatenate | solution.py:237
  3.0 3.2 %collective-permute-start.3 = (bf16[2048,256]{1,0:T(8,128)(2,1)}, bf16[2048,256]{1,0:T(8,128)(2,1)}, u32[]{:S(2)}, u32[]{:S(2)}) collective-permute-start(bf16[2048,256]{1,0:T(8,128)(2,1)} %pad_maximum_fusion.refs_0_), channel_id=1, source_target_pairs={{0,2},{2,0},{1,3},{3,1},{4,6},{6,4},{5,7},{7,5},{8,10},{10,8},{9,1... | collective-permute-start | bytes 3145736 | tf_op jit(solution)/shard_map/ppermute | solution.py:31
  6.3 1.7 %front.1 = bf16[256,2048]{1,0:T(8,128)(2,1)} custom-call(s32[1]{0:T(128)} %bitcast.40.member, bf16[128,2048]{1,0:T(8,128)(2,1)S(1)} %copy-done.1, f32[1,2048]{1,0:T(1,128)S(1)} %bitcast.130, s32[4,128]{1,0:T(4,128)S(1)} %bitcast.131), custom_call_target="tpu_custom_call" | custom-call | tf_op jit(solution)/shard_map/front/pallas_call | solution.py:141
  8.0 12.2 %all-to-all-start = ((bf16[32,8,2048]{2,1,0:T(8,128)(2,1)}), bf16[32,8,2048]{2,1,0:T(8,128)(2,1)S(1)}, u32[]{:S(2)}, u32[]{:S(2)}) async-start(bf16[32,8,2048]{2,1,0:T(8,128)(2,1)} %bitcast.44), calls=%async_computation | async-start | bytes 2097152 | tf_op jit(solution)/shard_map/all_to_all | solution.py:35
  20.2 2.1 %collective-permute-start.6 = (bf16[128,2048]{1,0:T(8,128)(2,1)S(1)}, bf16[128,2048]{1,0:T(8,128)(2,1)S(1)}, u32[]{:S(2)}, u32[]{:S(2)}) collective-permute-start(bf16[128,2048]{1,0:T(8,128)(2,1)S(1)} %bitcast.127), channel_id=1, source_target_pairs={{0,2},{2,0},{1,3},{3,1},{4,6},{6,4},{5,7},{7,5},{8,10},{10,8},{9,1... | collective-permute-start | bytes 1572872 | tf_op jit(solution)/shard_map/ppermute | solution.py:31
  22.3 3.7 %collective-permute-start.2 = (bf16[2048,256]{1,0:T(8,128)(2,1)}, bf16[2048,256]{1,0:T(8,128)(2,1)}, u32[]{:S(2)}, u32[]{:S(2)}) collective-permute-start(bf16[2048,256]{1,0:T(8,128)(2,1)} %pad_maximum_fusion.refs_0_), channel_id=1, source_target_pairs={{0,1},{1,0},{2,3},{3,2},{4,5},{5,4},{6,7},{7,6},{8,9},{9,8},{10,11... | collective-permute-start | bytes 3145736 | tf_op jit(solution)/shard_map/ppermute | solution.py:31
  26.0 3.3 %collective-permute-done.3.refs_2_ = bf16[2048,256]{1,0:T(8,128)(2,1)} collective-permute-done((bf16[2048,256]{1,0:T(8,128)(2,1)}, bf16[2048,256]{1,0:T(8,128)(2,1)}, u32[]{:S(2)}, u32[]{:S(2)}) %collective-permute-start.3) | collective-permute-done | bytes 1048608 | tf_op jit(solution)/shard_map/ppermute | solution.py:31
  29.3 4.6 %collective-permute-start.4 = (bf16[2048,256]{1,0:T(8,128)(2,1)}, bf16[2048,256]{1,0:T(8,128)(2,1)}, u32[]{:S(2)}, u32[]{:S(2)}) collective-permute-start(bf16[2048,256]{1,0:T(8,128)(2,1)} %collective-permute-done.3.refs_2_), channel_id=1, source_target_pairs={{0,1},{1,0},{2,3},{3,2},{4,5},{5,4},{6,7},{7,6},{8,9},{9,8},{10,11... | collective-permute-start | bytes 3145736 | tf_op jit(solution)/shard_map/ppermute | solution.py:31
  33.8 1.9 %collective-permute-start.5 = (bf16[128,2048]{1,0:T(8,128)(2,1)S(1)}, bf16[128,2048]{1,0:T(8,128)(2,1)S(1)}, u32[]{:S(2)}, u32[]{:S(2)}) collective-permute-start(bf16[128,2048]{1,0:T(8,128)(2,1)S(1)} %bitcast.128), channel_id=1, source_target_pairs={{0,1},{1,0},{2,3},{3,2},{4,5},{5,4},{6,7},{7,6},{8,9},{9,8},{10,11... | collective-permute-start | bytes 1572872 | tf_op jit(solution)/shard_map/ppermute | solution.py:31
  35.8 1.2 convert_reduce_fusion
  37.0 3.4 %collective-permute-done.6.refs_2_ = bf16[128,2048]{1,0:T(8,128)(2,1)S(1)} collective-permute-done((bf16[128,2048]{1,0:T(8,128)(2,1)S(1)}, bf16[128,2048]{1,0:T(8,128)(2,1)S(1)}, u32[]{:S(2)}, u32[]{:S(2)}) %collective-permute-start.6) | collective-permute-done | bytes 524320 | tf_op jit(solution)/shard_map/ppermute | solution.py:31
  40.4 3.4 %collective-permute-start.7 = (bf16[128,2048]{1,0:T(8,128)(2,1)S(1)}, bf16[128,2048]{1,0:T(8,128)(2,1)}, u32[]{:S(2)}, u32[]{:S(2)}) collective-permute-start(bf16[128,2048]{1,0:T(8,128)(2,1)S(1)} %collective-permute-done.6.refs_2_), channel_id=1, source_target_pairs={{0,1},{1,0},{2,3},{3,2},{4,5},{5,4},{6,7},{7,6},{8,9},{9,8},{10,11... | collective-permute-start | bytes 1572872 | tf_op jit(solution)/shard_map/ppermute | solution.py:31
  43.9 1.3 fusion.7
  45.2 0.0 collective-permute-done.2.refs_1_
  45.2 0.3 all-to-all-done
  45.5 0.0 collective-permute-done.4.refs_3_
  45.5 3.5 %shard_map.149.hidden_ref = bf16[256,512]{1,0:T(8,128)(2,1)S(1)} custom-call(bf16[256,2048]{1,0:T(8,128)(2,1)S(1)} %bitcast.126, bf16[2048,256]{1,0:T(8,128)(2,1)} %pad_maximum_fusion.refs_0_, bf16[2048,256]{1,0:T(8,128)(2,1)} %collective-permute-done.2.refs_1_, bf16[2048,256]{1,0:T(8,128)(2,1)} %collective-permute-done.3.refs_2_, ...), custom_call_target="tpu_custom_call" | custom-call | tf_op jit(solution)/shard_map/pallas_call | solution.py:206
  49.0 0.0 collective-permute-done.5.refs_1_
  49.0 0.0 collective-permute-done.7.refs_3_
  49.0 2.7 %shard_map.150 = bf16[256,2048]{1,0:T(8,128)(2,1)} custom-call(bf16[256,512]{1,0:T(8,128)(2,1)S(1)} %shard_map.149.hidden_ref, bf16[128,2048]{1,0:T(8,128)(2,1)S(1)} %bitcast.129, bf16[128,2048]{1,0:T(8,128)(2,1)S(1)} %collective-permute-done.5.refs_1_, bf16[128,2048]{1,0:T(8,128)(2,1)S(1)} %collective-permute-done.6.refs_2_, ...), custom_call_target="tpu_custom_call" | custom-call | tf_op jit(solution)/shard_map/pallas_call | solution.py:206
  51.8 11.8 %all-to-all-start.1 = ((bf16[32,8,2048]{2,1,0:T(8,128)(2,1)}), bf16[32,8,2048]{2,1,0:T(8,128)(2,1)S(1)}, u32[]{:S(2)}, u32[]{:S(2)}) async-start(bf16[32,8,2048]{2,1,0:T(8,128)(2,1)} %bitcast.134), calls=%async_computation.1 | async-start | bytes 2097152 | tf_op jit(solution)/shard_map/all_to_all | solution.py:35
  63.7 0.0 copy-start.10
  63.7 0.4 fusion.57
  64.1 0.6 copy-done.10
  64.7 0.4 fusion.6
  65.1 0.1 slice.272
  65.2 3.1 %collective-permute-start = (bf16[30,96]{0,1:T(8,128)(2,1)S(1)}, bf16[30,96]{0,1:T(8,128)(2,1)S(1)}, u32[]{:S(2)}, u32[]{:S(2)}) collective-permute-start(bf16[30,96]{0,1:T(8,128)(2,1)S(1)} %slice.272), channel_id=1, source_target_pairs={{0,16},{16,32},{32,48},{48,64},{64,80},{80,96},{96,112},{112,128},... | collective-permute-start | bytes 17288 | tf_op jit(solution)/shard_map/ppermute | solution.py:27
  68.3 0.3 mixing.1
  68.7 19.7 %collective-permute-done = bf16[30,96]{0,1:T(8,128)(2,1)S(1)} collective-permute-done((bf16[30,96]{0,1:T(8,128)(2,1)S(1)}, bf16[30,96]{0,1:T(8,128)(2,1)S(1)}, u32[]{:S(2)}, u32[]{:S(2)}) %collective-permute-start) | collective-permute-done | bytes 5792 | tf_op jit(solution)/shard_map/ppermute | solution.py:27
  88.4 0.9 fusion.59
  89.3 19.1 %all-gather.1 = f32[16,2,128]{2,1,0:T(2,128)S(1)} all-gather(f32[1,2,128]{2,1,0:T(2,128)S(1)} %maximum_bitcast_fusion), channel_id=2, replica_groups=mesh['ep'=32,'y2'=2,'y1'=2,'y0'=2,'c'=2] {'y2','y1','y0','c'}, dimensions={0}, use_global_device_ids=true | all-gather | bytes 17408 | tf_op jit(solution)/shard_map/all_gather | solution.py:92
  108.5 0.4 fusion.19
  108.9 2.1 %collective-permute-start.1 = (bf16[64,2048]{1,0:T(8,128)(2,1)S(1)}, bf16[64,2048]{1,0:T(8,128)(2,1)S(1)}, u32[]{:S(2)}, u32[]{:S(2)}) collective-permute-start(bf16[64,2048]{1,0:T(8,128)(2,1)S(1)} %fusion.15), channel_id=1, source_target_pairs={{0,1},{1,0},{2,3},{3,2},{4,5},{5,4},{6,7},{7,6},{8,9},{9,8},{10,11... | collective-permute-start | bytes 786440 | tf_op jit(solution)/shard_map/ppermute | solution.py:31
  111.0 0.3 fusion.10
  111.4 0.3 convolution_add_fusion
  111.7 2.3 %collective-permute-start.8 = (bf16[64,2048]{1,0:T(8,128)(2,1)S(1)}, bf16[64,2048]{1,0:T(8,128)(2,1)S(1)}, u32[]{:S(2)}, u32[]{:S(2)}) collective-permute-start(bf16[64,2048]{1,0:T(8,128)(2,1)S(1)} %fusion.16), channel_id=1, source_target_pairs={{0,1},{1,0},{2,3},{3,2},{4,5},{5,4},{6,7},{7,6},{8,9},{9,8},{10,11... | collective-permute-start | bytes 786440 | tf_op jit(solution)/shard_map/ppermute | solution.py:31
  114.0 0.1 fusion.17
  114.1 1.1 collective-permute-done.8
  115.2 0.1 fusion.18
  115.2 0.1 pad_maximum_fusion.1
  115.3 20.7 %all_to_all.20 = bf16[8,2,8,2048]{3,2,1,0:T(8,128)(2,1)S(1)} all-to-all(bf16[8,2,8,2048]{3,2,1,0:T(8,128)(2,1)S(1)} %pad_maximum_fusion.1), channel_id=1, replica_groups=mesh['ep'=32,'y2'=2,'y1'=2,'y0'=2,'c'=2] {'y2','y1','y0'}, dimensions={0} | all-to-all | bytes 1048576 | tf_op jit(solution)/shard_map/all_to_all | solution.py:35
  136.0 0.1 reduce_sum.62
  136.1 17.7 %all_to_all.21 = bf16[8,2,8,2048]{3,2,1,0:T(8,128)(2,1)S(1)} all-to-all(bf16[8,2,8,2048]{3,2,1,0:T(8,128)(2,1)S(1)} %broadcast_in_dim.2), channel_id=1, replica_groups=mesh['ep'=32,'y2'=2,'y1'=2,'y0'=2,'c'=2] {'y2','y1','y0'}, dimensions={0} | all-to-all | bytes 1048576 | tf_op jit(solution)/shard_map/all_to_all | solution.py:35
  153.9 5.0 %collective-permute-start.9 = (bf16[8,2,8,2048]{3,2,1,0:T(8,128)(2,1)S(1)}, bf16[8,2,8,2048]{3,2,1,0:T(8,128)(2,1)S(1)}, u32[]{:S(2)}, u32[]{:S(2)}) collective-permute-start(bf16[8,2,8,2048]{3,2,1,0:T(8,128)(2,1)S(1)} %all_to_all.21), channel_id=1, source_target_pairs={{0,1},{1,0},{2,3},{3,2},{4,5},{5,4},{6,7},{7,6},{8,9},{9,8},{10,11... | collective-permute-start | bytes 1572872 | tf_op jit(solution)/shard_map/ppermute | solution.py:31
  158.9 1.5 collective-permute-done.9
  160.4 0.1 select_bitcast_fusion.1
  160.5 1.0 pad_maximum_fusion.2
  (34 shorter events, 0.3 us)
Async XLA Ops:
  0.6 107.8 %copy-start = (bf16[96,2048]{1,0:T(8,128)(2,1)S(1)}, bf16[96,2048]{1,0:T(8,128)(2,1)}, u32[]{:S(2)}) copy-start(bf16[96,2048]{1,0:T(8,128)(2,1)} %param.20) | copy-start | bytes 1179652
  0.6 5.6 %copy-start.1 = (bf16[128,2048]{1,0:T(8,128)(2,1)S(1)}, bf16[128,2048]{1,0:T(8,128)(2,1)}, u32[]{:S(2)}) copy-start(bf16[128,2048]{1,0:T(8,128)(2,1)} %x_ref.1) | copy-start | bytes 1572868
  0.7 5.6 %copy-start.3 = (f32[2048]{0:T(1024)S(1)}, f32[2048]{0:T(1024)}, u32[]{:S(2)}) copy-start(f32[2048]{0:T(1024)} %param.22) | copy-start | bytes 24580
  0.7 5.6 %copy-start.4 = (s32[128,4]{0,1:T(4,128)S(1)}, s32[128,4]{0,1:T(4,128)}, u32[]{:S(2)}) copy-start(s32[128,4]{0,1:T(4,128)} %param.23) | copy-start | bytes 6148
  3.0 26.2 %collective-permute-start.3 = (bf16[2048,256]{1,0:T(8,128)(2,1)}, bf16[2048,256]{1,0:T(8,128)(2,1)}, u32[]{:S(2)}, u32[]{:S(2)}) collective-permute-start(bf16[2048,256]{1,0:T(8,128)(2,1)} %pad_maximum_fusion.refs_0_), channel_id=1, source_target_pairs={{0,2},{2,0},{1,3},{3,1},{4,6},{6,4},{5,7},{7,5},{8,10},{10,8},{9,1... | collective-permute-start | bytes 3145736 | tf_op jit(solution)/shard_map/ppermute | solution.py:31
  8.0 12.2 %copy-start.2 = (bf16[1,128,2048]{2,1,0:T(8,128)(2,1)S(1)}, bf16[1,128,2048]{2,1,0:T(8,128)(2,1)}, u32[]{:S(2)}) copy-start(bf16[1,128,2048]{2,1,0:T(8,128)(2,1)} %param.27) | copy-start | bytes 1572868
  8.0 37.5 %all-to-all-start = ((bf16[32,8,2048]{2,1,0:T(8,128)(2,1)}), bf16[32,8,2048]{2,1,0:T(8,128)(2,1)S(1)}, u32[]{:S(2)}, u32[]{:S(2)}) async-start(bf16[32,8,2048]{2,1,0:T(8,128)(2,1)} %bitcast.44), calls=%async_computation | async-start | bytes 2097152 | tf_op jit(solution)/shard_map/all_to_all | solution.py:35
  20.2 20.2 %collective-permute-start.6 = (bf16[128,2048]{1,0:T(8,128)(2,1)S(1)}, bf16[128,2048]{1,0:T(8,128)(2,1)S(1)}, u32[]{:S(2)}, u32[]{:S(2)}) collective-permute-start(bf16[128,2048]{1,0:T(8,128)(2,1)S(1)} %bitcast.127), channel_id=1, source_target_pairs={{0,2},{2,0},{1,3},{3,1},{4,6},{6,4},{5,7},{7,5},{8,10},{10,8},{9,1... | collective-permute-start | bytes 1572872 | tf_op jit(solution)/shard_map/ppermute | solution.py:31
  22.3 22.9 %collective-permute-start.2 = (bf16[2048,256]{1,0:T(8,128)(2,1)}, bf16[2048,256]{1,0:T(8,128)(2,1)}, u32[]{:S(2)}, u32[]{:S(2)}) collective-permute-start(bf16[2048,256]{1,0:T(8,128)(2,1)} %pad_maximum_fusion.refs_0_), channel_id=1, source_target_pairs={{0,1},{1,0},{2,3},{3,2},{4,5},{5,4},{6,7},{7,6},{8,9},{9,8},{10,11... | collective-permute-start | bytes 3145736 | tf_op jit(solution)/shard_map/ppermute | solution.py:31
  29.3 16.3 %collective-permute-start.4 = (bf16[2048,256]{1,0:T(8,128)(2,1)}, bf16[2048,256]{1,0:T(8,128)(2,1)}, u32[]{:S(2)}, u32[]{:S(2)}) collective-permute-start(bf16[2048,256]{1,0:T(8,128)(2,1)} %collective-permute-done.3.refs_2_), channel_id=1, source_target_pairs={{0,1},{1,0},{2,3},{3,2},{4,5},{5,4},{6,7},{7,6},{8,9},{9,8},{10,11... | collective-permute-start | bytes 3145736 | tf_op jit(solution)/shard_map/ppermute | solution.py:31
  33.8 15.2 %collective-permute-start.5 = (bf16[128,2048]{1,0:T(8,128)(2,1)S(1)}, bf16[128,2048]{1,0:T(8,128)(2,1)S(1)}, u32[]{:S(2)}, u32[]{:S(2)}) collective-permute-start(bf16[128,2048]{1,0:T(8,128)(2,1)S(1)} %bitcast.128), channel_id=1, source_target_pairs={{0,1},{1,0},{2,3},{3,2},{4,5},{5,4},{6,7},{7,6},{8,9},{9,8},{10,11... | collective-permute-start | bytes 1572872 | tf_op jit(solution)/shard_map/ppermute | solution.py:31
  40.4 8.6 %collective-permute-start.7 = (bf16[128,2048]{1,0:T(8,128)(2,1)S(1)}, bf16[128,2048]{1,0:T(8,128)(2,1)}, u32[]{:S(2)}, u32[]{:S(2)}) collective-permute-start(bf16[128,2048]{1,0:T(8,128)(2,1)S(1)} %collective-permute-done.6.refs_2_), channel_id=1, source_target_pairs={{0,1},{1,0},{2,3},{3,2},{4,5},{5,4},{6,7},{7,6},{8,9},{9,8},{10,11... | collective-permute-start | bytes 1572872 | tf_op jit(solution)/shard_map/ppermute | solution.py:31
  51.8 11.9 %copy-start.6 = (bf16[128,2048]{1,0:T(8,128)(2,1)S(1)}, bf16[128,2048]{1,0:T(8,128)(2,1)}, u32[]{:S(2)}) copy-start(bf16[128,2048]{1,0:T(8,128)(2,1)} %param.14) | copy-start | bytes 1572868
  51.8 11.9 %copy-start.9 = (bf16[2048,96]{0,1:T(8,128)(2,1)S(1)}, bf16[2048,96]{0,1:T(8,128)(2,1)}, u32[]{:S(2)}) copy-start(bf16[2048,96]{0,1:T(8,128)(2,1)} %param.16) | copy-start | bytes 1179652
  51.8 11.9 %copy-start.11 = (f32[2048]{0:T(1024)S(1)}, f32[2048]{0:T(1024)}, u32[]{:S(2)}) copy-start(f32[2048]{0:T(1024)} %param.15) | copy-start | bytes 24580
  51.8 59.2 %all-to-all-start.1 = ((bf16[32,8,2048]{2,1,0:T(8,128)(2,1)}), bf16[32,8,2048]{2,1,0:T(8,128)(2,1)S(1)}, u32[]{:S(2)}, u32[]{:S(2)}) async-start(bf16[32,8,2048]{2,1,0:T(8,128)(2,1)} %bitcast.134), calls=%async_computation.1 | async-start | bytes 2097152 | tf_op jit(solution)/shard_map/all_to_all | solution.py:35
  63.7 1.0 copy-start.10
  64.7 3.6 %copy-start.7 = (f32[31,96]{1,0:T(8,128)S(1)}, f32[31,96]{1,0:T(8,128)}, u32[]{:S(2)}) copy-start(f32[31,96]{1,0:T(8,128)} %param.18) | copy-start | bytes 35716
  64.7 3.7 %copy-start.5 = (f32[128,4]{0,1:T(4,128)S(1)}, f32[128,4]{0,1:T(4,128)}, u32[]{:S(2)}) copy-start(f32[128,4]{0,1:T(4,128)} %param.24) | copy-start | bytes 6148
  64.7 43.8 %copy-start.8 = (f32[96]{0:T(128)S(1)}, f32[96]{0:T(128)}, u32[]{:S(2)}) copy-start(f32[96]{0:T(128)} %param.19) | copy-start | bytes 1156
  65.2 23.2 %collective-permute-start = (bf16[30,96]{0,1:T(8,128)(2,1)S(1)}, bf16[30,96]{0,1:T(8,128)(2,1)S(1)}, u32[]{:S(2)}, u32[]{:S(2)}) collective-permute-start(bf16[30,96]{0,1:T(8,128)(2,1)S(1)} %slice.272), channel_id=1, source_target_pairs={{0,16},{16,32},{32,48},{48,64},{64,80},{80,96},{96,112},{112,128},... | collective-permute-start | bytes 17288 | tf_op jit(solution)/shard_map/ppermute | solution.py:27
  108.9 5.1 %collective-permute-start.1 = (bf16[64,2048]{1,0:T(8,128)(2,1)S(1)}, bf16[64,2048]{1,0:T(8,128)(2,1)S(1)}, u32[]{:S(2)}, u32[]{:S(2)}) collective-permute-start(bf16[64,2048]{1,0:T(8,128)(2,1)S(1)} %fusion.15), channel_id=1, source_target_pairs={{0,1},{1,0},{2,3},{3,2},{4,5},{5,4},{6,7},{7,6},{8,9},{9,8},{10,11... | collective-permute-start | bytes 786440 | tf_op jit(solution)/shard_map/ppermute | solution.py:31
  111.7 3.4 %collective-permute-start.8 = (bf16[64,2048]{1,0:T(8,128)(2,1)S(1)}, bf16[64,2048]{1,0:T(8,128)(2,1)S(1)}, u32[]{:S(2)}, u32[]{:S(2)}) collective-permute-start(bf16[64,2048]{1,0:T(8,128)(2,1)S(1)} %fusion.16), channel_id=1, source_target_pairs={{0,1},{1,0},{2,3},{3,2},{4,5},{5,4},{6,7},{7,6},{8,9},{9,8},{10,11... | collective-permute-start | bytes 786440 | tf_op jit(solution)/shard_map/ppermute | solution.py:31
  153.9 6.6 %collective-permute-start.9 = (bf16[8,2,8,2048]{3,2,1,0:T(8,128)(2,1)S(1)}, bf16[8,2,8,2048]{3,2,1,0:T(8,128)(2,1)S(1)}, u32[]{:S(2)}, u32[]{:S(2)}) collective-permute-start(bf16[8,2,8,2048]{3,2,1,0:T(8,128)(2,1)S(1)} %all_to_all.21), channel_id=1, source_target_pairs={{0,1},{1,0},{2,3},{3,2},{4,5},{5,4},{6,7},{7,6},{8,9},{9,8},{10,11... | collective-permute-start | bytes 1572872 | tf_op jit(solution)/shard_map/ppermute | solution.py:31

commit v4 on v3

--- a/solution.py
+++ b/solution.py
@@ -143,7 +143,7 @@
         in_specs=[pl.BlockSpec(memory_space=pltpu.SMEM)] + [whole] * 3,
         out_specs=whole,
         out_shape=jax.ShapeDtypeStruct((sent, width), jnp.bfloat16),
-        compiler_params=pltpu.CompilerParams(vmem_limit_bytes=8 << 20),
+        compiler_params=pltpu.CompilerParams(vmem_limit_bytes=60 * 1024 * 1024),
         name="front",
     )(member.reshape(1), x, gain.reshape(1, width), ids)
 
@@ -181,10 +181,11 @@
 
 
 def hidden_kernel(x_ref, *refs):
-    gus, out_ref = refs[:GROUP], refs[GROUP]
-    inner = gus[0].shape[1] // 2
-    for at, gu in enumerate(gus):
-        both = jnp.dot(x_ref[...], gu[...], preferred_element_type=jnp.float32)
+    gates, ups, out_ref = refs[:GROUP], refs[GROUP : 2 * GROUP], refs[2 * GROUP]
+    inner = gates[0].shape[1]
+    for at, (gate, up) in enumerate(zip(gates, ups, strict=True)):
+        weights = jnp.concatenate([gate[...], up[...]], axis=1)
+        both = jnp.dot(x_ref[...], weights, preferred_element_type=jnp.float32)
         g = jnp.minimum(both[:, :inner], clamp_limit)
         u = jnp.clip(both[:, inner:], -clamp_limit, clamp_limit)
         hidden = (u + 1.0) * g * jax.nn.sigmoid(swish_slope * g)
@@ -234,14 +235,12 @@
     slots = capacity // GROUP
     member = lax.axis_index(("y0", "c")).astype(jnp.int32)
 
-    gate_up = jnp.concatenate([expert_gate[0], expert_up[0]], axis=1)
-    down = expert_down[0]
-    gu_y = swapped(gate_up, "y0")
-    down_y = swapped(down, "y0")
-    gu_c = swapped(gate_up, "c")
-    down_c = swapped(down, "c")
-    gu_d = swapped(gu_y, "c")
-    down_d = swapped(down_y, "c")
+    own = {"gate": expert_gate[0], "up": expert_up[0], "down": expert_down[0]}
+    weights = {name: [w] for name, w in own.items()}
+    for name, w in own.items():
+        weights[name].append(swapped(w, "c"))
+        near = swapped(w, "y0")
+        weights[name] += [near, swapped(near, "c")]
 
     ids = route_experts.T
     sending = front(member, expert_in, expert_gain, ids, experts * slots)
@@ -252,9 +251,10 @@
     mixer_partial = projected(conv_out, channel_gain, w_output)
     mixer_half = core_half(mixer_partial)
 
-    hidden_shape = (experts * slots, GROUP * down.shape[0])
-    hidden = in_vmem(hidden_kernel, 53000, hidden_shape, arrived, gate_up, gu_c, gu_y, gu_d)
-    partial = in_vmem(down_kernel, 53000, arrived.shape, hidden, down, down_c, down_y, down_d)
+    hidden_shape = (experts * slots, GROUP * own["down"].shape[0])
+    pairs = (arrived, *weights["gate"], *weights["up"])
+    hidden = in_vmem(hidden_kernel, 53000, hidden_shape, *pairs)
+    partial = in_vmem(down_kernel, 53000, arrived.shape, hidden, *weights["down"])
     returned = exchanged(partial.reshape(experts, slots, width), "ep").reshape(-1, width)
 
     def mixed(m):

time: 162 us -> 173 us (1.068)
  starting transfers between devices: 55.3 us -> 65.2 us
  other arithmetic: 7.15 us -> 2.7 us
  local copies, waits for them, and re-layouts: 0.86 us -> 3.75 us
    ppermute x9 -> x12, starting transfers between devices: 28.2 us -> 40.6 us  [swapped(): return lax.ppermute(x, axis, [(0, 1), (1, 0)])]
    unnamed x24 -> x32, local copies, waits for them, and re-layouts: 0.64 us -> 3.53 us
    ppermute x9 -> x12, waiting for transfers between devices: 9.33 us -> 11.9 us  [swapped(): return lax.ppermute(x, axis, [(0, 1), (1, 0)])]
    all_to_all x2, starting transfers between devices: 24 us -> 21.6 us  [exchanged(): return lax.all_to_all(x, axis, split_axis=0, concat_axis=0, tiled=True)]
    concatenate x1 -> x0, other arithmetic: 2.36 us -> none  [program(): gate_up = jnp.concatenate([expert_gate[0], expert_up[0]], axis=1)]
  transfers between devices with their start and end apart: 12 -> 15, of which waited for: 6 -> 5; matrix products, arithmetic and copies ran while one was open for 3% -> 2% of each run, Pallas kernels for 3% -> 2%
where the time goes in v4:
time: 173 us; the launch traced here: 172 us
  starting transfers between devices  65.2 us (38%)
  blocking collectives  57.6 us (33%)
  waiting for transfers between devices  30.9 us (18%)
  Pallas kernels  9.23 us (5%)
  local copies, waits for them, and re-layouts  3.75 us (2%)
  other arithmetic  2.7 us (2%)
  matrix products  1.87 us (1%)
    ppermute x12, starting transfers between devices, swapped(): return lax.ppermute(x, axis, [(0, 1), (1, 0)])  40.6 us
    all_to_all x2, blocking collectives, exchanged(): return lax.all_to_all(x, axis, split_axis=0, concat_axis=0, tiled=True)  38.4 us
    all_to_all x2, starting transfers between devices, exchanged(): return lax.all_to_all(x, axis, split_axis=0, concat_axis=0, tiled=True)  21.6 us
    all_gather x1, blocking collectives, projected(): everyone = lax.all_gather(sums, TP)  19.1 us
    ppermute x1, waiting for transfers between devices, shifted(): return lax.ppermute(block, axis, route)  19.1 us
    ppermute x12, waiting for transfers between devices, swapped(): return lax.ppermute(x, axis, [(0, 1), (1, 0)])  11.9 us
    pallas_call x2, Pallas kernels, in_vmem(): pl.pallas_call(kernel, in_specs=[whole] * len(operands), out_specs=whole,...  6.02 us
    unnamed x32, local copies, waits for them, and re-layouts  3.53 us
  transfers between devices with their start and end apart: 15, of which 5 were waited for; matrix products, arithmetic and copies ran while one was open for 2% of the time, Pallas kernels for 2%

profile of v4, /device:TPU:65, one launch (start us, length us, event | category | flops | bytes accessed | tf_op | source)
XLA Modules:
  0.0 172.4 jit_solution(755337020909001351)
XLA Ops:
  0.7 2.9 %front.1 = bf16[256,2048]{1,0:T(8,128)(2,1)} custom-call(s32[1]{0:T(128)} %bitcast.40.member, bf16[128,2048]{1,0:T(8,128)(2,1)} %x_ref.1, f32[1,2048]{1,0:T(1,128)} %bitcast.141, s32[4,128]{1,0:T(4,128)} %bitcast.132), custom_call_target="tpu_custom_call" | custom-call | tf_op jit(solution)/shard_map/front/pallas_call | solution.py:141
  3.5 12.2 %all-to-all-start = ((bf16[32,8,2048]{2,1,0:T(8,128)(2,1)}), bf16[32,8,2048]{2,1,0:T(8,128)(2,1)}, u32[]{:S(2)}, u32[]{:S(2)}) async-start(bf16[32,8,2048]{2,1,0:T(8,128)(2,1)} %bitcast.136), calls=%async_computation | async-start | bytes 2097152 | tf_op jit(solution)/shard_map/all_to_all | solution.py:35
  15.8 3.3 %collective-permute-start.3 = (bf16[2048,128]{1,0:T(8,128)(2,1)S(1)}, bf16[2048,128]{1,0:T(8,128)(2,1)S(1)}, u32[]{:S(2)}, u32[]{:S(2)}) collective-permute-start(bf16[2048,128]{1,0:T(8,128)(2,1)S(1)} %bitcast.129), channel_id=1, source_target_pairs={{0,2},{2,0},{1,3},{3,1},{4,6},{6,4},{5,7},{7,5},{8,10},{10,8},{9,1... | collective-permute-start | bytes 1572872 | tf_op jit(solution)/shard_map/ppermute | solution.py:31
  19.1 2.1 %collective-permute-start.6 = (bf16[2048,128]{1,0:T(8,128)(2,1)}, bf16[2048,128]{1,0:T(8,128)(2,1)S(1)}, u32[]{:S(2)}, u32[]{:S(2)}) collective-permute-start(bf16[2048,128]{1,0:T(8,128)(2,1)} %bitcast.47.refs_4_), channel_id=1, source_target_pairs={{0,2},{2,0},{1,3},{3,1},{4,6},{6,4},{5,7},{7,5},{8,10},{10,8},{9,1... | collective-permute-start | bytes 1572872 | tf_op jit(solution)/shard_map/ppermute | solution.py:31
  21.2 3.7 %collective-permute-start.2 = (bf16[2048,128]{1,0:T(8,128)(2,1)S(1)}, bf16[2048,128]{1,0:T(8,128)(2,1)S(1)}, u32[]{:S(2)}, u32[]{:S(2)}) collective-permute-start(bf16[2048,128]{1,0:T(8,128)(2,1)S(1)} %bitcast.130), channel_id=1, source_target_pairs={{0,1},{1,0},{2,3},{3,2},{4,5},{5,4},{6,7},{7,6},{8,9},{9,8},{10,11... | collective-permute-start | bytes 1572872 | tf_op jit(solution)/shard_map/ppermute | solution.py:31
  24.9 3.2 %collective-permute-start.9 = (bf16[128,2048]{1,0:T(8,128)(2,1)S(1)}, bf16[128,2048]{1,0:T(8,128)(2,1)S(1)}, u32[]{:S(2)}, u32[]{:S(2)}) collective-permute-start(bf16[128,2048]{1,0:T(8,128)(2,1)S(1)} %bitcast.126), channel_id=1, source_target_pairs={{0,2},{2,0},{1,3},{3,1},{4,6},{6,4},{5,7},{7,5},{8,10},{10,8},{9,1... | collective-permute-start | bytes 1572872 | tf_op jit(solution)/shard_map/ppermute | solution.py:31
  28.2 2.2 %collective-permute-start.5 = (bf16[2048,128]{1,0:T(8,128)(2,1)}, bf16[2048,128]{1,0:T(8,128)(2,1)S(1)}, u32[]{:S(2)}, u32[]{:S(2)}) collective-permute-start(bf16[2048,128]{1,0:T(8,128)(2,1)} %bitcast.47.refs_4_), channel_id=1, source_target_pairs={{0,1},{1,0},{2,3},{3,2},{4,5},{5,4},{6,7},{7,6},{8,9},{9,8},{10,11... | collective-permute-start | bytes 1572872 | tf_op jit(solution)/shard_map/ppermute | solution.py:31
  30.4 0.2 convert_reduce_fusion
  30.5 5.2 %collective-permute-start.8 = (bf16[128,2048]{1,0:T(8,128)(2,1)S(1)}, bf16[128,2048]{1,0:T(8,128)(2,1)S(1)}, u32[]{:S(2)}, u32[]{:S(2)}) collective-permute-start(bf16[128,2048]{1,0:T(8,128)(2,1)S(1)} %bitcast.127), channel_id=1, source_target_pairs={{0,1},{1,0},{2,3},{3,2},{4,5},{5,4},{6,7},{7,6},{8,9},{9,8},{10,11... | collective-permute-start | bytes 1572872 | tf_op jit(solution)/shard_map/ppermute | solution.py:31
  35.8 5.6 %collective-permute-done.6.refs_6_ = bf16[2048,128]{1,0:T(8,128)(2,1)S(1)} collective-permute-done((bf16[2048,128]{1,0:T(8,128)(2,1)}, bf16[2048,128]{1,0:T(8,128)(2,1)S(1)}, u32[]{:S(2)}, u32[]{:S(2)}) %collective-permute-start.6) | collective-permute-done | bytes 524320 | tf_op jit(solution)/shard_map/ppermute | solution.py:31
  41.4 5.6 %collective-permute-start.4 = (bf16[2048,128]{1,0:T(8,128)(2,1)S(1)}, bf16[2048,128]{1,0:T(8,128)(2,1)S(1)}, u32[]{:S(2)}, u32[]{:S(2)}) collective-permute-start(bf16[2048,128]{1,0:T(8,128)(2,1)S(1)} %collective-permute-done.3.refs_2_), channel_id=1, source_target_pairs={{0,1},{1,0},{2,3},{3,2},{4,5},{5,4},{6,7},{7,6},{8,9},{9,8},{10,11... | collective-permute-start | bytes 1572872 | tf_op jit(solution)/shard_map/ppermute | solution.py:31
  47.0 1.9 %collective-permute-start.7 = (bf16[2048,128]{1,0:T(8,128)(2,1)S(1)}, bf16[2048,128]{1,0:T(8,128)(2,1)}, u32[]{:S(2)}, u32[]{:S(2)}) collective-permute-start(bf16[2048,128]{1,0:T(8,128)(2,1)S(1)} %collective-permute-done.6.refs_6_), channel_id=1, source_target_pairs={{0,1},{1,0},{2,3},{3,2},{4,5},{5,4},{6,7},{7,6},{8,9},{9,8},{10,11... | collective-permute-start | bytes 1572872 | tf_op jit(solution)/shard_map/ppermute | solution.py:31
  48.9 3.6 %collective-permute-done.9.refs_2_ = bf16[128,2048]{1,0:T(8,128)(2,1)S(1)} collective-permute-done((bf16[128,2048]{1,0:T(8,128)(2,1)S(1)}, bf16[128,2048]{1,0:T(8,128)(2,1)S(1)}, u32[]{:S(2)}, u32[]{:S(2)}) %collective-permute-start.9) | collective-permute-done | bytes 524320 | tf_op jit(solution)/shard_map/ppermute | solution.py:31
  52.5 4.0 %collective-permute-start.10 = (bf16[128,2048]{1,0:T(8,128)(2,1)S(1)}, bf16[128,2048]{1,0:T(8,128)(2,1)}, u32[]{:S(2)}, u32[]{:S(2)}) collective-permute-start(bf16[128,2048]{1,0:T(8,128)(2,1)S(1)} %collective-permute-done.9.refs_2_), channel_id=1, source_target_pairs={{0,1},{1,0},{2,3},{3,2},{4,5},{5,4},{6,7},{7,6},{8,9},{9,8},{10,11... | collective-permute-start | bytes 1572872 | tf_op jit(solution)/shard_map/ppermute | solution.py:31
  56.6 0.3 fusion.7
  56.9 0.8 copy-done.9
  57.7 0.8 copy-done.10
  58.5 3.3 %shard_map.149.hidden_ref = bf16[256,512]{1,0:T(8,128)(2,1)S(1)} custom-call(bf16[256,2048]{1,0:T(8,128)(2,1)} %bitcast.45.x_ref, bf16[2048,128]{1,0:T(8,128)(2,1)S(1)} %bitcast.131, bf16[2048,128]{1,0:T(8,128)(2,1)S(1)} %collective-permute-done.2.refs_1_, bf16[2048,128]{1,0:T(8,128)(2,1)S(1)} %collective-permute-done.3.refs_2_, ...), custom_call_target="tpu_custom_call" | custom-call | tf_op jit(solution)/shard_map/pallas_call | solution.py:207
  61.8 2.7 %shard_map.150 = bf16[256,2048]{1,0:T(8,128)(2,1)} custom-call(bf16[256,512]{1,0:T(8,128)(2,1)S(1)} %shard_map.149.hidden_ref, bf16[128,2048]{1,0:T(8,128)(2,1)S(1)} %bitcast.128, bf16[128,2048]{1,0:T(8,128)(2,1)S(1)} %collective-permute-done.8.refs_1_, bf16[128,2048]{1,0:T(8,128)(2,1)S(1)} %collective-permute-done.9.refs_2_, ...), custom_call_target="tpu_custom_call" | custom-call | tf_op jit(solution)/shard_map/pallas_call | solution.py:207
  64.5 9.3 %all-to-all-start.1 = ((bf16[32,8,2048]{2,1,0:T(8,128)(2,1)}), bf16[32,8,2048]{2,1,0:T(8,128)(2,1)S(1)}, u32[]{:S(2)}, u32[]{:S(2)}) async-start(bf16[32,8,2048]{2,1,0:T(8,128)(2,1)} %bitcast.135), calls=%async_computation.1 | async-start | bytes 2097152 | tf_op jit(solution)/shard_map/all_to_all | solution.py:35
  73.9 0.4 fusion.57
  74.3 0.6 copy-done.14
  74.9 0.4 fusion.6
  75.3 0.1 slice.272
  75.4 3.1 %collective-permute-start = (bf16[30,96]{0,1:T(8,128)(2,1)S(1)}, bf16[30,96]{0,1:T(8,128)(2,1)S(1)}, u32[]{:S(2)}, u32[]{:S(2)}) collective-permute-start(bf16[30,96]{0,1:T(8,128)(2,1)S(1)} %slice.272), channel_id=1, source_target_pairs={{0,16},{16,32},{32,48},{48,64},{64,80},{80,96},{96,112},{112,128},... | collective-permute-start | bytes 17288 | tf_op jit(solution)/shard_map/ppermute | solution.py:27
  78.6 0.6 copy-done.4
  79.2 0.0 copy-done.3
  79.2 0.3 mixing.1
  79.6 19.1 %collective-permute-done = bf16[30,96]{0,1:T(8,128)(2,1)S(1)} collective-permute-done((bf16[30,96]{0,1:T(8,128)(2,1)S(1)}, bf16[30,96]{0,1:T(8,128)(2,1)S(1)}, u32[]{:S(2)}, u32[]{:S(2)}) %collective-permute-start) | collective-permute-done | bytes 5792 | tf_op jit(solution)/shard_map/ppermute | solution.py:27
  98.6 0.9 fusion.59
  99.5 19.1 %all-gather.1 = f32[16,2,128]{2,1,0:T(2,128)S(1)} all-gather(f32[1,2,128]{2,1,0:T(2,128)S(1)} %maximum_bitcast_fusion), channel_id=2, replica_groups=mesh['ep'=32,'y2'=2,'y1'=2,'y0'=2,'c'=2] {'y2','y1','y0','c'}, dimensions={0}, use_global_device_ids=true | all-gather | bytes 17408 | tf_op jit(solution)/shard_map/all_gather | solution.py:92
  118.7 0.6 copy-done.12
  119.3 0.4 fusion.19
  119.8 2.1 %collective-permute-start.1 = (bf16[64,2048]{1,0:T(8,128)(2,1)S(1)}, bf16[64,2048]{1,0:T(8,128)(2,1)S(1)}, u32[]{:S(2)}, u32[]{:S(2)}) collective-permute-start(bf16[64,2048]{1,0:T(8,128)(2,1)S(1)} %fusion.15), channel_id=1, source_target_pairs={{0,1},{1,0},{2,3},{3,2},{4,5},{5,4},{6,7},{7,6},{8,9},{9,8},{10,11... | collective-permute-start | bytes 786440 | tf_op jit(solution)/shard_map/ppermute | solution.py:31
  121.9 0.3 fusion.10
  122.2 0.3 convolution_add_fusion
  122.6 2.2 %collective-permute-start.11 = (bf16[64,2048]{1,0:T(8,128)(2,1)S(1)}, bf16[64,2048]{1,0:T(8,128)(2,1)S(1)}, u32[]{:S(2)}, u32[]{:S(2)}) collective-permute-start(bf16[64,2048]{1,0:T(8,128)(2,1)S(1)} %fusion.16), channel_id=1, source_target_pairs={{0,1},{1,0},{2,3},{3,2},{4,5},{5,4},{6,7},{7,6},{8,9},{9,8},{10,11... | collective-permute-start | bytes 786440 | tf_op jit(solution)/shard_map/ppermute | solution.py:31
  124.9 0.1 fusion.17
  124.9 1.1 collective-permute-done.11
  126.0 0.1 fusion.18
  126.1 0.1 pad_maximum_fusion
  126.2 20.7 %all_to_all.20 = bf16[8,2,8,2048]{3,2,1,0:T(8,128)(2,1)S(1)} all-to-all(bf16[8,2,8,2048]{3,2,1,0:T(8,128)(2,1)S(1)} %pad_maximum_fusion), channel_id=1, replica_groups=mesh['ep'=32,'y2'=2,'y1'=2,'y0'=2,'c'=2] {'y2','y1','y0'}, dimensions={0} | all-to-all | bytes 1048576 | tf_op jit(solution)/shard_map/all_to_all | solution.py:35
  146.9 0.1 reduce_sum.62
  147.0 17.7 %all_to_all.21 = bf16[8,2,8,2048]{3,2,1,0:T(8,128)(2,1)S(1)} all-to-all(bf16[8,2,8,2048]{3,2,1,0:T(8,128)(2,1)S(1)} %broadcast_in_dim.2), channel_id=1, replica_groups=mesh['ep'=32,'y2'=2,'y1'=2,'y0'=2,'c'=2] {'y2','y1','y0'}, dimensions={0} | all-to-all | bytes 1048576 | tf_op jit(solution)/shard_map/all_to_all | solution.py:35
  164.7 5.0 %collective-permute-start.12 = (bf16[8,2,8,2048]{3,2,1,0:T(8,128)(2,1)S(1)}, bf16[8,2,8,2048]{3,2,1,0:T(8,128)(2,1)S(1)}, u32[]{:S(2)}, u32[]{:S(2)}) collective-permute-start(bf16[8,2,8,2048]{3,2,1,0:T(8,128)(2,1)S(1)} %all_to_all.21), channel_id=1, source_target_pairs={{0,1},{1,0},{2,3},{3,2},{4,5},{5,4},{6,7},{7,6},{8,9},{9,8},{10,11... | collective-permute-start | bytes 1572872 | tf_op jit(solution)/shard_map/ppermute | solution.py:31
  169.8 1.5 collective-permute-done.12
  171.3 0.1 select_bitcast_fusion.1
  171.4 1.0 pad_maximum_fusion.1
  (47 shorter events, 0.3 us)
Async XLA Ops:
  0.6 118.1 %copy-start = (bf16[96,2048]{1,0:T(8,128)(2,1)S(1)}, bf16[96,2048]{1,0:T(8,128)(2,1)}, u32[]{:S(2)}) copy-start(bf16[96,2048]{1,0:T(8,128)(2,1)} %param.20) | copy-start | bytes 1179652
  3.5 12.2 %copy-start.2 = (bf16[1,2048,128]{2,1,0:T(8,128)(2,1)S(1)}, bf16[1,2048,128]{2,1,0:T(8,128)(2,1)}, u32[]{:S(2)}) copy-start(bf16[1,2048,128]{2,1,0:T(8,128)(2,1)} %param.25) | copy-start | bytes 1572868
  3.5 21.4 %copy-start.1 = (bf16[1,128,2048]{2,1,0:T(8,128)(2,1)S(1)}, bf16[1,128,2048]{2,1,0:T(8,128)(2,1)}, u32[]{:S(2)}) copy-start(bf16[1,128,2048]{2,1,0:T(8,128)(2,1)} %param.27) | copy-start | bytes 1572868
  3.5 26.8 %copy-start.5 = (bf16[128,2048]{1,0:T(8,128)(2,1)S(1)}, bf16[128,2048]{1,0:T(8,128)(2,1)}, u32[]{:S(2)}) copy-start(bf16[128,2048]{1,0:T(8,128)(2,1)} %param.14) | copy-start | bytes 1572868
  3.5 54.9 %all-to-all-start = ((bf16[32,8,2048]{2,1,0:T(8,128)(2,1)}), bf16[32,8,2048]{2,1,0:T(8,128)(2,1)}, u32[]{:S(2)}, u32[]{:S(2)}) async-start(bf16[32,8,2048]{2,1,0:T(8,128)(2,1)} %bitcast.136), calls=%async_computation | async-start | bytes 2097152 | tf_op jit(solution)/shard_map/all_to_all | solution.py:35
  15.8 40.8 %copy-start.6 = (bf16[128,2048]{1,0:T(8,128)(2,1)S(1)}, bf16[128,2048]{1,0:T(8,128)(2,1)}, u32[]{:S(2)}) copy-start(bf16[128,2048]{1,0:T(8,128)(2,1)} %param.14) | copy-start | bytes 1572868
  15.8 14.7 %collective-permute-start.3 = (bf16[2048,128]{1,0:T(8,128)(2,1)S(1)}, bf16[2048,128]{1,0:T(8,128)(2,1)S(1)}, u32[]{:S(2)}, u32[]{:S(2)}) collective-permute-start(bf16[2048,128]{1,0:T(8,128)(2,1)S(1)} %bitcast.129), channel_id=1, source_target_pairs={{0,2},{2,0},{1,3},{3,1},{4,6},{6,4},{5,7},{7,5},{8,10},{10,8},{9,1... | collective-permute-start | bytes 1572872 | tf_op jit(solution)/shard_map/ppermute | solution.py:31
  19.1 22.3 %collective-permute-start.6 = (bf16[2048,128]{1,0:T(8,128)(2,1)}, bf16[2048,128]{1,0:T(8,128)(2,1)S(1)}, u32[]{:S(2)}, u32[]{:S(2)}) collective-permute-start(bf16[2048,128]{1,0:T(8,128)(2,1)} %bitcast.47.refs_4_), channel_id=1, source_target_pairs={{0,2},{2,0},{1,3},{3,1},{4,6},{6,4},{5,7},{7,5},{8,10},{10,8},{9,1... | collective-permute-start | bytes 1572872 | tf_op jit(solution)/shard_map/ppermute | solution.py:31
  21.2 25.8 %collective-permute-start.2 = (bf16[2048,128]{1,0:T(8,128)(2,1)S(1)}, bf16[2048,128]{1,0:T(8,128)(2,1)S(1)}, u32[]{:S(2)}, u32[]{:S(2)}) collective-permute-start(bf16[2048,128]{1,0:T(8,128)(2,1)S(1)} %bitcast.130), channel_id=1, source_target_pairs={{0,1},{1,0},{2,3},{3,2},{4,5},{5,4},{6,7},{7,6},{8,9},{9,8},{10,11... | collective-permute-start | bytes 1572872 | tf_op jit(solution)/shard_map/ppermute | solution.py:31
  24.9 27.6 %collective-permute-start.9 = (bf16[128,2048]{1,0:T(8,128)(2,1)S(1)}, bf16[128,2048]{1,0:T(8,128)(2,1)S(1)}, u32[]{:S(2)}, u32[]{:S(2)}) collective-permute-start(bf16[128,2048]{1,0:T(8,128)(2,1)S(1)} %bitcast.126), channel_id=1, source_target_pairs={{0,2},{2,0},{1,3},{3,1},{4,6},{6,4},{5,7},{7,5},{8,10},{10,8},{9,1... | collective-permute-start | bytes 1572872 | tf_op jit(solution)/shard_map/ppermute | solution.py:31
  28.2 28.7 %collective-permute-start.5 = (bf16[2048,128]{1,0:T(8,128)(2,1)}, bf16[2048,128]{1,0:T(8,128)(2,1)S(1)}, u32[]{:S(2)}, u32[]{:S(2)}) collective-permute-start(bf16[2048,128]{1,0:T(8,128)(2,1)} %bitcast.47.refs_4_), channel_id=1, source_target_pairs={{0,1},{1,0},{2,3},{3,2},{4,5},{5,4},{6,7},{7,6},{8,9},{9,8},{10,11... | collective-permute-start | bytes 1572872 | tf_op jit(solution)/shard_map/ppermute | solution.py:31
  30.5 31.2 %collective-permute-start.8 = (bf16[128,2048]{1,0:T(8,128)(2,1)S(1)}, bf16[128,2048]{1,0:T(8,128)(2,1)S(1)}, u32[]{:S(2)}, u32[]{:S(2)}) collective-permute-start(bf16[128,2048]{1,0:T(8,128)(2,1)S(1)} %bitcast.127), channel_id=1, source_target_pairs={{0,1},{1,0},{2,3},{3,2},{4,5},{5,4},{6,7},{7,6},{8,9},{9,8},{10,11... | collective-permute-start | bytes 1572872 | tf_op jit(solution)/shard_map/ppermute | solution.py:31
  41.4 15.5 %copy-start.8 = (bf16[2048,128]{1,0:T(8,128)(2,1)}, bf16[2048,128]{1,0:T(8,128)(2,1)S(1)}, u32[]{:S(2)}) copy-start(bf16[2048,128]{1,0:T(8,128)(2,1)S(1)} %collective-permute-done.6.refs_6_) | copy-start | bytes 1572868
  41.4 15.5 %collective-permute-start.4 = (bf16[2048,128]{1,0:T(8,128)(2,1)S(1)}, bf16[2048,128]{1,0:T(8,128)(2,1)S(1)}, u32[]{:S(2)}, u32[]{:S(2)}) collective-permute-start(bf16[2048,128]{1,0:T(8,128)(2,1)S(1)} %collective-permute-done.3.refs_2_), channel_id=1, source_target_pairs={{0,1},{1,0},{2,3},{3,2},{4,5},{5,4},{6,7},{7,6},{8,9},{9,8},{10,11... | collective-permute-start | bytes 1572872 | tf_op jit(solution)/shard_map/ppermute | solution.py:31
  47.0 11.4 %collective-permute-start.7 = (bf16[2048,128]{1,0:T(8,128)(2,1)S(1)}, bf16[2048,128]{1,0:T(8,128)(2,1)}, u32[]{:S(2)}, u32[]{:S(2)}) collective-permute-start(bf16[2048,128]{1,0:T(8,128)(2,1)S(1)} %collective-permute-done.6.refs_6_), channel_id=1, source_target_pairs={{0,1},{1,0},{2,3},{3,2},{4,5},{5,4},{6,7},{7,6},{8,9},{9,8},{10,11... | collective-permute-start | bytes 1572872 | tf_op jit(solution)/shard_map/ppermute | solution.py:31
  52.5 9.2 %collective-permute-start.10 = (bf16[128,2048]{1,0:T(8,128)(2,1)S(1)}, bf16[128,2048]{1,0:T(8,128)(2,1)}, u32[]{:S(2)}, u32[]{:S(2)}) collective-permute-start(bf16[128,2048]{1,0:T(8,128)(2,1)S(1)} %collective-permute-done.9.refs_2_), channel_id=1, source_target_pairs={{0,1},{1,0},{2,3},{3,2},{4,5},{5,4},{6,7},{7,6},{8,9},{9,8},{10,11... | collective-permute-start | bytes 1572872 | tf_op jit(solution)/shard_map/ppermute | solution.py:31
  56.9 0.8 copy-start.9
  57.7 0.8 copy-start.10
  64.5 9.4 %copy-start.7 = (bf16[128,2048]{1,0:T(8,128)(2,1)S(1)}, bf16[128,2048]{1,0:T(8,128)(2,1)}, u32[]{:S(2)}) copy-start(bf16[128,2048]{1,0:T(8,128)(2,1)} %param.14) | copy-start | bytes 1572868
  64.5 9.4 %copy-start.13 = (bf16[2048,96]{0,1:T(8,128)(2,1)S(1)}, bf16[2048,96]{0,1:T(8,128)(2,1)}, u32[]{:S(2)}) copy-start(bf16[2048,96]{0,1:T(8,128)(2,1)} %param.16) | copy-start | bytes 1179652
  64.5 9.4 %copy-start.15 = (f32[2048]{0:T(1024)S(1)}, f32[2048]{0:T(1024)}, u32[]{:S(2)}) copy-start(f32[2048]{0:T(1024)} %param.15) | copy-start | bytes 24580
  64.5 57.4 %all-to-all-start.1 = ((bf16[32,8,2048]{2,1,0:T(8,128)(2,1)}), bf16[32,8,2048]{2,1,0:T(8,128)(2,1)S(1)}, u32[]{:S(2)}, u32[]{:S(2)}) async-start(bf16[32,8,2048]{2,1,0:T(8,128)(2,1)} %bitcast.135), calls=%async_computation.1 | async-start | bytes 2097152 | tf_op jit(solution)/shard_map/all_to_all | solution.py:35
  73.9 1.0 copy-start.14
  75.3 3.2 %copy-start.11 = (f32[31,96]{1,0:T(8,128)S(1)}, f32[31,96]{1,0:T(8,128)}, u32[]{:S(2)}) copy-start(f32[31,96]{1,0:T(8,128)} %param.18) | copy-start | bytes 35716
  75.4 23.2 %collective-permute-start = (bf16[30,96]{0,1:T(8,128)(2,1)S(1)}, bf16[30,96]{0,1:T(8,128)(2,1)S(1)}, u32[]{:S(2)}, u32[]{:S(2)}) collective-permute-start(bf16[30,96]{0,1:T(8,128)(2,1)S(1)} %slice.272), channel_id=1, source_target_pairs={{0,16},{16,32},{32,48},{48,64},{64,80},{80,96},{96,112},{112,128},... | collective-permute-start | bytes 17288 | tf_op jit(solution)/shard_map/ppermute | solution.py:27
  78.5 0.7 copy-start.4
  78.6 0.7 copy-start.3
  118.7 0.7 copy-start.12
  119.8 5.1 %collective-permute-start.1 = (bf16[64,2048]{1,0:T(8,128)(2,1)S(1)}, bf16[64,2048]{1,0:T(8,128)(2,1)S(1)}, u32[]{:S(2)}, u32[]{:S(2)}) collective-permute-start(bf16[64,2048]{1,0:T(8,128)(2,1)S(1)} %fusion.15), channel_id=1, source_target_pairs={{0,1},{1,0},{2,3},{3,2},{4,5},{5,4},{6,7},{7,6},{8,9},{9,8},{10,11... | collective-permute-start | bytes 786440 | tf_op jit(solution)/shard_map/ppermute | solution.py:31
  122.6 3.4 %collective-permute-start.11 = (bf16[64,2048]{1,0:T(8,128)(2,1)S(1)}, bf16[64,2048]{1,0:T(8,128)(2,1)S(1)}, u32[]{:S(2)}, u32[]{:S(2)}) collective-permute-start(bf16[64,2048]{1,0:T(8,128)(2,1)S(1)} %fusion.16), channel_id=1, source_target_pairs={{0,1},{1,0},{2,3},{3,2},{4,5},{5,4},{6,7},{7,6},{8,9},{9,8},{10,11... | collective-permute-start | bytes 786440 | tf_op jit(solution)/shard_map/ppermute | solution.py:31
  164.7 6.6 %collective-permute-start.12 = (bf16[8,2,8,2048]{3,2,1,0:T(8,128)(2,1)S(1)}, bf16[8,2,8,2048]{3,2,1,0:T(8,128)(2,1)S(1)}, u32[]{:S(2)}, u32[]{:S(2)}) collective-permute-start(bf16[8,2,8,2048]{3,2,1,0:T(8,128)(2,1)S(1)} %all_to_all.21), channel_id=1, source_target_pairs={{0,1},{1,0},{2,3},{3,2},{4,5},{5,4},{6,7},{7,6},{8,9},{9,8},{10,11... | collective-permute-start | bytes 1572872 | tf_op jit(solution)/shard_map/ppermute | solution.py:31
